TPU v7x, 32 devices: a whole 2x2x4 slice. The times are simulated.
32 devices in a mesh: fs: 8 (over z, x), tp: 4 (over y, core).
Axes of the slice: x: 2, y: 2, z: 4, core: 2. Of those that a mesh axis runs over, the one named last changes fastest.
Arguments:
- tokens: bfloat16 [1024, 2048], P('fs', 'tp'), may hold values from -6 to 6
- routes: int32 [1024, 2], P('fs'), may hold values from 0 to 3, all different within a row; in each aligned block of 128 rows (0 to 127, 128 to 255, ...) at most 96 rows name the same one
- route_weight: float32 [1024, 2], P('fs'), may hold values from 0.1 to 1
- norm_gain: float32 [2048], P('fs'), may hold values from 0.1 to 1.9
- expert_gate: float32 [4, 2048, 512], P(None, 'fs', 'tp'), may hold values from -0.125 to 0.125
- expert_up: float32 [4, 2048, 512], P(None, 'fs', 'tp'), may hold values from -0.125 to 0.125
- expert_down: float32 [4, 2048, 512], P(None, 'fs', 'tp'), may hold values from -0.25 to 0.25
- shared_gate: float32 [2048, 512], P('fs', 'tp'), may hold values from -0.125 to 0.125
- shared_up: float32 [2048, 512], P('fs', 'tp'), may hold values from -0.125 to 0.125
- shared_down: float32 [512, 2048], P('tp', 'fs'), may hold values from -0.25 to 0.25
Outputs:
- mixed: bfloat16 [1024, 2048], P('fs', 'tp')
- gate_sampler: bfloat16 [8, 2048, 256], P('fs', None, 'tp')
- up_sampler: bfloat16 [8, 2048, 256], P('fs', None, 'tp')
- down_sampler: bfloat16 [8, 2048, 256], P('fs', 'tp')
- shared_gate_out: bfloat16 [2048, 512], P(None, 'tp')
- shared_up_out: bfloat16 [2048, 512], P(None, 'tp')
- shared_down_out: bfloat16 [512, 2048], P('tp')
Inputs may be any that keep to these rules, and one draw needn't show every extreme that they name: `routes`: each row names 2 different experts. In each aligned block of 128 rows no expert is named by more than 96 rows, a bound that some block reaches.
All inputs are finite; a program needn't handle non-finite values.
Results may differ from a plain program's by a relative error of at most 0.009.
Values may be sent and summed in bfloat16 or wider, within the bound.
A program may use at most 64 MiB of HBM per device.

v0:
```python
import functools

import jax
import jax.numpy as jnp
from jax import lax
from jax.experimental import pallas as pl
from jax.experimental.pallas import tpu as pltpu
from jax.sharding import PartitionSpec as P

EPS = 1e-06
BF = jnp.bfloat16
F32 = jnp.float32


def loop(low, high, body):
    def step(i, carry):
        body(i)
        return carry

    lax.fori_loop(low, high, step, 0)


def dot(a, b):
    return jnp.dot(a, b, preferred_element_type=F32)


def dot_nt(a, b):
    return lax.dot_general(a, b, (((1,), (1,)), ((), ())), preferred_element_type=F32)


def left_halves(a, b, half):
    lane = lax.broadcasted_iota(jnp.int32, a.shape, 1)
    return jnp.where(lane < half, a, pltpu.roll(b, half, 1))


def right_halves(a, b, half):
    lane = lax.broadcasted_iota(jnp.int32, a.shape, 1)
    return jnp.where(lane < half, pltpu.roll(a, half, 1), b)


def silu(v):
    return v / (1.0 + jnp.exp(-v))


def kernel(
    F,
    T,
    slots,
    tok,
    routes,
    weight,
    gain,
    eg,
    eu,
    ed,
    sg,
    su,
    sd,
    mixed,
    gate_out,
    up_out,
    dn_out,
    sg_out,
    su_out,
    sd_out,
    tk,
    nm,
    gu_send,
    gu,
    dn_send,
    dn,
    sh,
    disp,
    port,
    hid,
    away,
    keep,
    near,
    ret_send,
    ret,
    part,
    shr,
    s_tok,
    r_tok,
    s_gu,
    r_gu,
    s_dn,
    r_dn,
    s_left,
    s_right,
    s_shb,
    r_sh,
    s_da,
    s_db,
    s_out,
    s_in,
    r_port,
    s_hid,
    r_hid,
    s_near,
    r_near,
    s_ret,
    r_ret,
    s_shr,
    r_shr,
):
    G = F // 2
    K = F // T
    E = eg.shape[0]
    R, C = eg.shape[1], eg.shape[2]
    half = C // 2
    tok_count = tok.shape[0]
    quarter = tok.shape[1]
    width = quarter * T
    f = lax.axis_index("fs")
    t = lax.axis_index("tp")
    g, p = f // 2, f % 2
    pair = g * 2 + (1 - p)
    t_pair = (t // 2) * 2 + (1 - t % 2)

    def remote(src, dst, send, recv, fs, tp):
        return pltpu.make_async_remote_copy(
            src_ref=src,
            dst_ref=dst,
            send_sem=send,
            recv_sem=recv,
            device_id={"fs": fs, "tp": tp},
            device_id_type=pl.DeviceIdType.MESH,
        )

    def arrived(dst, send, recv):
        remote(dst, dst, send, recv, pair, t).wait_recv()

    def sent(src, send, recv):
        remote(src, src, send, recv, pair, t).wait_send()

    def tok_copy(src, sem, to):
        return remote(tk.at[src], tk.at[src], sem, r_tok.at[src], f, to)

    for o in range(1, T // 2):
        remote(tok, tk.at[t], s_tok.at[o], r_tok.at[t], f, (t + 2 * o) % T).start()
    remote(tok, tk.at[t], s_tok.at[T // 2], r_tok.at[t], f, t_pair).start()
    tk[t] = tok[...]

    experts = lax.broadcasted_iota(jnp.int32, (tok_count, E), 1)
    line = lax.broadcasted_iota(jnp.int32, (8, tok_count), 0)
    named_by = routes[...].astype(F32)
    turned = jnp.where(line == 0, named_by[0:1], named_by[1:2])
    turned = jnp.where(line == 2, weight[0:1, :], turned)
    turned = jnp.where(line == 3, weight[1:2, :], turned).T
    first, second = turned[:, 0:1].astype(jnp.int32), turned[:, 1:2].astype(jnp.int32)
    named = ((experts == first) | (experts == second)).astype(F32)
    rows = lax.broadcasted_iota(jnp.int32, (tok_count, tok_count), 0)
    cols = lax.broadcasted_iota(jnp.int32, (tok_count, tok_count), 1)
    before = (cols < rows).astype(F32).astype(BF)
    place = dot(before, named.astype(BF))
    slot_ids = lax.broadcasted_iota(jnp.int32, (tok_count, E * slots), 1)

    def pick_of(chosen):
        spot = jnp.sum(jnp.where(experts == chosen, place, 0.0), axis=1, keepdims=True)
        return slot_ids == chosen * slots + spot.astype(jnp.int32)

    pick0, pick1 = pick_of(first), pick_of(second)
    both = jnp.where(pick0 | pick1, 1.0, 0.0).astype(BF)

    packed = lax.dot_general(
        both, tok[...], (((0,), (0,)), ((), ())), preferred_element_type=F32
    ).astype(BF)
    disp[...] = packed.reshape(E, slots, quarter)
    port[t, f] = disp[g]

    def send_disp(d):
        e = (g + d) % G
        remote(
            disp.at[e], port.at[t, f], s_da.at[d], r_port.at[t, f], 2 * e + p, t
        ).start()

    loop(1, G, send_disp)

    def shared_copy(block, sems, to):
        return remote(sh.at[block], sh.at[block], sems, r_sh.at[block], to, t)

    def share_left(block):
        @pl.when(g > 0)
        def _():
            shared_copy(block, s_left.at[block // 2], f - 2).start()

    def share_right(block):
        @pl.when(g < G - 1)
        def _():
            shared_copy(block, s_right.at[block // 2], f + 2).start()

    def share_pair(block):
        shared_copy(block, s_shb.at[block // 2], pair).start()

    def relay(k):
        @pl.when(g - k >= 0)
        def _():
            block = f - 2 * k
            arrived(sh.at[block], s_right.at[0], r_sh.at[block])
            share_right(block)
            share_pair(block)

        @pl.when(g + k < G)
        def _():
            block = f + 2 * k
            arrived(sh.at[block], s_left.at[0], r_sh.at[block])
            share_left(block)
            share_pair(block)

    def pass_block(block):
        for d in range(1, T // 2):
            remote(
                port.at[t, block],
                port.at[t, block],
                s_out.at[d, block],
                r_port.at[t, block],
                f,
                (t + 2 * d) % T,
            ).start()
        remote(
            port.at[t, block],
            port.at[t, block],
            s_in.at[0, block],
            r_port.at[t, block],
            f,
            t_pair,
        ).start()

    def direct_block(d):
        block = ((g + G - d) % G) * 2 + p

        @pl.when(d > 0)
        def _():
            arrived(port.at[t, block], s_da.at[d], r_port.at[t, block])

        remote(
            port.at[t, block],
            port.at[t, block],
            s_db.at[d],
            r_port.at[t, block],
            pair,
            t,
        ).start()
        pass_block(block)

    def pair_block(d):
        block = ((g + G - d) % G) * 2 + 1 - p
        arrived(port.at[t, block], s_db.at[d], r_port.at[t, block])
        pass_block(block)

    def inner_block(d):
        for o in range(1, T // 2):
            src = (t + 2 * o) % T
            for q in (p, 1 - p):
                block = ((g + G - d) % G) * 2 + q
                arrived(port.at[src, block], s_out.at[o, block], r_port.at[src, block])
                remote(
                    port.at[src, block],
                    port.at[src, block],
                    s_in.at[o, block],
                    r_port.at[src, block],
                    f,
                    t_pair,
                ).start()

    loop(0, 1, direct_block)

    gains = jnp.broadcast_to(gain[...], (8, R)).T[:, 0:1]

    def fold(e):
        gate, up = eg[e] * gains, eu[e] * gains
        gu_send[2 * e] = left_halves(gate, up, half).astype(BF)
        gu_send[2 * e + 1] = right_halves(gate, up, half).astype(BF)

    loop(0, E, fold)
    gu[f] = gu_send[f]

    def send_gu(d):
        j = (f + d) % F
        remote(gu_send.at[j], gu.at[f], s_gu.at[d], r_gu.at[f], j, t).start()

    loop(1, F, send_gu)

    def fold_down(e):
        top, low = ed[e, : R // 2], ed[e, R // 2 :]
        dn_send[2 * e] = left_halves(top, low, half).astype(BF)
        dn_send[2 * e + 1] = right_halves(top, low, half).astype(BF)

    loop(0, E, fold_down)
    sh[f, 0] = (sg[...] * gains).astype(BF)
    sh[f, 1] = (su[...] * gains).astype(BF)
    sh[f, 2] = sd[...].T.astype(BF)

    def down_copy(d):
        j = (f + d) % F
        return remote(
            dn_send.at[j], dn.at[f % K, t], s_dn.at[d], r_dn.at[f % K, t], j, f // K
        )

    mine = f // K == t

    @pl.when(mine)
    def _():
        dn[f % K, t] = dn_send[f]

    def send_down(d):
        @pl.when(jnp.logical_not((d == 0) & mine))
        def _():
            down_copy(d).start()

    loop(0, F, send_down)
    share_left(f)
    share_right(f)
    loop(1, G, direct_block)
    loop(0, G, pair_block)
    share_pair(f)
    loop(0, G, inner_block)

    for o in range(1, T // 2):
        src = (t + 2 * o) % T
        arrived(tk.at[src], s_tok.at[o], r_tok.at[src])
        tok_copy(src, s_tok.at[T // 2 + o], t_pair).start()

    def wait_gu(d):
        src = (f + d) % F
        arrived(gu.at[src], s_gu.at[d], r_gu.at[src])

    loop(1, F, wait_gu)

    def rows_of(q):
        return gu[q * K : (q + 1) * K].reshape(quarter, C)

    def hidden_of(block):
        total = jnp.zeros((slots, C), F32)
        squares = jnp.zeros((slots, 1), F32)
        for q in range(T):
            total = total + dot(port[q, block], rows_of(q))
            x = port[q, block].astype(F32)
            squares = squares + jnp.sum(x * x, axis=1, keepdims=True)
        total = total * lax.rsqrt(squares / width + EPS)
        return silu(total) * pltpu.roll(total, half, 1)

    def wait_inner(block):
        for o in range(T // 2):
            src = (t_pair + 2 * o) % T
            arrived(port.at[src, block], s_in.at[o, block], r_port.at[src, block])

    def expert_hidden(d):
        group = (g + G - d) % G
        wait_inner(2 * group)
        wait_inner(2 * group + 1)
        hid[t, group] = left_halves(
            hidden_of(2 * group), hidden_of(2 * group + 1), half
        ).astype(BF)
        for o in range(1, T):
            remote(
                hid.at[t, group],
                hid.at[t, group],
                s_hid.at[o, group],
                r_hid.at[t, group],
                f,
                (t + o) % T,
            ).start()

    loop(0, G, expert_hidden)

    loop(1, min(2, G), relay)

    def wait_down(k):
        for q in range(T):

            @pl.when(jnp.logical_not((t * K + k == f) & (t == q)))
            def _():
                arrived(dn.at[k, q], s_dn.at[0], r_dn.at[k, q])

    loop(0, K, wait_down)

    def place_down(k):
        for q in range(0, T, 2):
            a, b = dn[k, q].astype(F32), dn[k, q + 1].astype(F32)
            block = jnp.concatenate([left_halves(a, b, half), right_halves(a, b, half)], axis=0)
            dn_out[pl.ds(pl.multiple_of(k * R, R), R), q * half : (q + 2) * half] = block.astype(BF)

    loop(0, K, place_down)

    def near_copy(group):
        return remote(
            away.at[group], near.at[group], s_near.at[group], r_near.at[group], pair, t
        )

    def expert_out(d):
        group = (g + G - d) % G
        for o in range(1, T):
            src = (t + o) % T
            arrived(hid.at[src, group], s_hid.at[o, group], r_hid.at[src, group])
        out_a = jnp.zeros((slots, quarter), F32)
        out_b = jnp.zeros((slots, quarter), F32)
        for q in range(0, T, 2):
            a, b = hid[q, group].astype(F32), hid[q + 1, group].astype(F32)
            down = dn_out[:, q * half : (q + 2) * half]
            out_a = out_a + dot_nt(left_halves(a, b, half).astype(BF), down)
            out_b = out_b + dot_nt(right_halves(a, b, half).astype(BF), down)
        even, odd = out_a.astype(BF), out_b.astype(BF)
        keep[group] = jnp.where(p == 0, even, odd)
        away[group] = jnp.where(p == 0, odd, even)
        near_copy(group).start()

    loop(0, G, expert_out)
    loop(2, min(3, G), relay)

    def add_halves(d):
        group = (g + d) % G
        arrived(near.at[group], s_near.at[group], r_near.at[group])
        ret_send[group] = (keep[group].astype(F32) + near[group].astype(F32)).astype(BF)
        remote(
            ret_send.at[group], ret.at[g], s_ret.at[group], r_ret.at[g], 2 * group + p, t
        ).start()

    loop(1, G, add_halves)
    arrived(near.at[g], s_near.at[g], r_near.at[g])
    ret[g] = (keep[g].astype(F32) + near[g].astype(F32)).astype(BF)

    def wait_shared(d):
        block = ((g + G - d) % G) * 2 + 1 - p
        arrived(sh.at[block], s_shb.at[d], r_sh.at[block])

    loop(3, G, relay)
    loop(0, G, wait_shared)

    for o in range(T // 2):
        src = (t_pair + 2 * o) % T
        arrived(tk.at[src], s_tok.at[o], r_tok.at[src])
    squares = jnp.zeros((tok_count, 1), F32)
    for q in range(T):
        x = tk[q].astype(F32)
        squares = squares + jnp.sum(x * x, axis=1, keepdims=True)
    scale = lax.rsqrt(squares / width + EPS)
    for q in range(T):
        nm[q] = (tk[q].astype(F32) * scale).astype(BF)

    gate_sh = sh[:, 0].reshape(F * R, C)
    up_sh = sh[:, 1].reshape(F * R, C)
    down_sh = sh[:, 2].reshape(F * R, C)
    act = jnp.zeros((tok_count, C), F32)
    lin = jnp.zeros((tok_count, C), F32)
    for q in range(T):
        act = act + dot(nm[q], gate_sh[q * quarter : (q + 1) * quarter])
        lin = lin + dot(nm[q], up_sh[q * quarter : (q + 1) * quarter])
    hidden_sh = (silu(act) * lin).astype(BF)
    for q in range(T):
        part[q] = dot_nt(hidden_sh, down_sh[q * quarter : (q + 1) * quarter]).astype(BF)
    shr[t] = part[t]

    def send_part(d):
        q = (t + d) % T
        remote(part.at[q], shr.at[t], s_shr.at[d], r_shr.at[t], f, q).start()

    loop(1, T, send_part)

    for q in range(T):
        span = slice(q * quarter, (q + 1) * quarter)
        turned_gu = rows_of(q).astype(F32).T.astype(BF)
        gate_out[:, span] = turned_gu[:half]
        up_out[:, span] = turned_gu[half:]
        sd_out[:, span] = (
            sh[q * K : (q + 1) * K, 2].reshape(quarter, C).astype(F32).T.astype(BF)
        )
    sg_out[...] = sh[:, 0].reshape(F * R, C)
    su_out[...] = sh[:, 1].reshape(F * R, C)

    def wait_part(d):
        src = (t + d) % T
        arrived(shr.at[src], s_shr.at[d], r_shr.at[src])

    loop(1, T, wait_part)
    total = shr[0].astype(F32)
    for q in range(1, T):
        total = total + shr[q].astype(F32)

    def wait_ret(d):
        src = (g + d) % G
        arrived(ret.at[src], s_ret.at[src], r_ret.at[src])

    loop(1, G, wait_ret)
    outs = ret[...].reshape(E * slots, quarter)
    for k, pick in enumerate((pick0, pick1)):
        chosen = jnp.where(pick, 1.0, 0.0).astype(BF)
        total = total + turned[:, 2 + k : 3 + k] * dot(chosen, outs)
    mixed[...] = total.astype(BF)

    def done_tp(d):
        sent(tok, s_tok.at[d], r_tok.at[0])
        sent(part.at[0], s_shr.at[d], r_shr.at[0])

        def inner(group):
            sent(hid.at[t, group], s_hid.at[d, group], r_hid.at[0, 0])

        loop(0, G, inner)

    loop(1, T, done_tp)

    def done_fs(d):
        sent(gu_send.at[0], s_gu.at[d], r_gu.at[0])

    loop(1, F, done_fs)

    def done_down(d):
        @pl.when(jnp.logical_not((d == 0) & mine))
        def _():
            sent(dn_send.at[0], s_dn.at[d], r_dn.at[0, 0])

    loop(0, F, done_down)

    def done_groups(d):
        sent(sh.at[f], s_shb.at[d], r_sh.at[0])
        sent(disp.at[0], s_db.at[d], r_port.at[0, 0])
        sent(away.at[0], s_near.at[d], r_near.at[0])

        @pl.when(d > 0)
        def _():
            sent(disp.at[0], s_da.at[d], r_port.at[0, 0])
            sent(ret_send.at[0], s_ret.at[(g + d) % G], r_ret.at[0])

        @pl.when((d >= g) & (g > 0))
        def _():
            sent(sh.at[f], s_left.at[d], r_sh.at[0])

        @pl.when((d <= g) & (g < G - 1))
        def _():
            sent(sh.at[f], s_right.at[d], r_sh.at[0])

    loop(0, G, done_groups)

    def done_blocks(block):
        for o in range(T // 2):
            sent(disp.at[0], s_in.at[o, block], r_port.at[0, 0])
            if o > 0:
                sent(disp.at[0], s_out.at[o, block], r_port.at[0, 0])

    loop(0, F, done_blocks)


def hand_on(count, *refs):
    for i in range(count):
        refs[count + i][...] = refs[i][...]


def on_device(
    tokens,
    routes,
    route_weight,
    norm_gain,
    expert_gate,
    expert_up,
    expert_down,
    shared_gate,
    shared_up,
    shared_down,
):
    F = lax.axis_size("fs")
    T = lax.axis_size("tp")
    E, R, C = expert_gate.shape
    tok_count, quarter = tokens.shape
    pick_count = routes.shape[1]
    capacity = 2 * ((3 * tok_count * pick_count + 4 * E - 1) // (4 * E))
    slots = (capacity + 15) // 16 * 16
    G, K = F // 2, F // T
    vmem = pl.BlockSpec(memory_space=pltpu.VMEM)
    dma = pltpu.SemaphoreType.DMA
    shapes = [
        (tok_count, quarter),
        (C // 2, F * R),
        (C // 2, F * R),
        (K * R, T * C // 2),
        (F * R, C),
        (F * R, C),
        (C, F * R),
    ]
    scratch = [
        (T, tok_count, quarter),
        (T, tok_count, quarter),
        (F, R, C),
        (F, R, C),
        (F, R // 2, C),
        (K, T, R // 2, C),
        (F, 3, R, C),
        (E, slots, quarter),
        (T, F, slots, quarter),
        (T, G, slots, C),
        (G, slots, quarter),
        (G, slots, quarter),
        (G, slots, quarter),
        (G, slots, quarter),
        (E, slots, quarter),
        (T, tok_count, quarter),
        (T, tok_count, quarter),
    ]
    sems = [
        (T,), (T,), (F,), (F,), (F,), (K, T), (G,), (G,), (G,), (F,), (G,), (G,),
        (T // 2, F), (T // 2, F), (T, F), (T, G), (T, G), (G,), (G,), (G,), (E,), (T,), (T,),
    ]
    results = pl.pallas_call(
        functools.partial(kernel, F, T, slots),
        out_shape=[jax.ShapeDtypeStruct(s, BF) for s in shapes],
        in_specs=[vmem] * 10,
        out_specs=[vmem] * 7,
        scratch_shapes=[pltpu.VMEM(s, BF) for s in scratch] + [dma(s) for s in sems],
        compiler_params=pltpu.CompilerParams(
            has_side_effects=True, vmem_limit_bytes=60 * 1024 * 1024
        ),
    )(
        tokens,
        routes.T,
        route_weight.T,
        norm_gain[None, :],
        expert_gate,
        expert_up,
        expert_down,
        shared_gate,
        shared_up,
        shared_down,
    )
    mixed, gate, up, down, sg, su, sd = pl.pallas_call(
        functools.partial(hand_on, 7),
        out_shape=[jax.ShapeDtypeStruct(s, BF) for s in shapes],
        in_specs=[vmem] * 7,
        out_specs=[vmem] * 7,
    )(*results)
    return (mixed, gate.T[None], up.T[None], down[None], sg, su, sd)


def solution(mesh):
    in_specs = (
        P("fs", "tp"),
        P("fs", None),
        P("fs", None),
        P("fs"),
        P(None, "fs", "tp"),
        P(None, "fs", "tp"),
        P(None, "fs", "tp"),
        P("fs", "tp"),
        P("fs", "tp"),
        P("tp", "fs"),
    )
    out_specs = (
        P("fs", "tp"),
        P("fs", None, "tp"),
        P("fs", None, "tp"),
        P("fs", "tp", None),
        P(None, "tp"),
        P(None, "tp"),
        P("tp", None),
    )
    return jax.shard_map(
        on_device, mesh=mesh, in_specs=in_specs, out_specs=out_specs, check_vma=False
    )
```

profile of v0, /device:TPU:9, one launch (start us, length us, event | category | flops | bytes accessed | tf_op | source)
XLA Modules:
  0.0 79.9 jit_solution(15918554749897285184)
XLA Ops:
  0.6 76.2 %shard_map.153 = (bf16[128,512]{1,0:T(8,128)(2,1)}, bf16[64,2048]{1,0:T(8,128)(2,1)}, bf16[64,2048]{1,0:T(8,128)(2,1)}, bf16[512,256]{1,0:T(8,128)(2,1)}, bf16[2...) custom-call(bf16[128,512]{1,0:T(8,128)(2,1)} %tok.1, s32[2,128]{1,0:T(2,128)} %bitcast.10, ...), custom_call_target="tpu_custom_call" | custom-call | tf_op jit(solution)/shard_map/pallas_call | solution.py:603
  76.8 3.1 %shard_map.154 = (bf16[128,512]{1,0:T(8,128)(2,1)}, bf16[64,2048]{1,0:T(8,128)(2,1)}, bf16[64,2048]{1,0:T(8,128)(2,1)}, bf16[512,256]{1,0:T(8,128)(2,1)}, bf16[2...) custom-call(bf16[128,512]{1,0:T(8,128)(2,1)} %get-tuple-element.21.refs_0_, ...), custom_call_target="tpu_custom_call" | custom-call | tf_op jit(solution)/shard_map/pallas_call | solution.py:624
where the time goes:
time: 80.1 us; the launch traced here: 79.9 us
  Pallas kernels  79.3 us (99%)
    pallas_call x1, Pallas kernels, on_device(): pl.pallas_call(functools.partial(kernel, F, T, slots), out_shape=[jax.Sha...  76.2 us
    pallas_call x1, Pallas kernels, on_device(): pl.pallas_call(functools.partial(hand_on, 7), out_shape=[jax.ShapeDtypeSt...  3.1 us

commit v1 on v0

--- a/solution.py
+++ b/solution.py
@@ -46,6 +46,23 @@
     F,
     T,
     slots,
+    tok_in,
+    routes_in,
+    weight_in,
+    gain_in,
+    eg_in,
+    eu_in,
+    ed_in,
+    sg_in,
+    su_in,
+    sd_in,
+    mixed,
+    gate_out,
+    up_out,
+    dn_out,
+    sg_out,
+    su_out,
+    sd_out,
     tok,
     routes,
     weight,
@@ -56,13 +73,7 @@
     sg,
     su,
     sd,
-    mixed,
-    gate_out,
-    up_out,
-    dn_out,
-    sg_out,
-    su_out,
-    sd_out,
+    s_load,
     tk,
     nm,
     gu_send,
@@ -137,11 +148,57 @@
     def tok_copy(src, sem, to):
         return remote(tk.at[src], tk.at[src], sem, r_tok.at[src], f, to)
 
+    loads = [
+        pltpu.make_async_copy(src, dst, s_load.at[i])
+        for i, (src, dst) in enumerate(
+            (
+                (tok_in, tok),
+                (routes_in, routes),
+                (weight_in, weight),
+                (gain_in, gain),
+                (eg_in, eg),
+                (eu_in, eu),
+                (ed_in, ed),
+                (sg_in, sg),
+                (su_in, su),
+                (sd_in, sd),
+            )
+        )
+    ]
+    for load in loads:
+        load.start()
+
+    barrier = pltpu.get_barrier_semaphore()
+
+    def greet(fs, tp):
+        pl.semaphore_signal(
+            barrier,
+            inc=1,
+            device_id={"fs": fs, "tp": tp},
+            device_id_type=pl.DeviceIdType.MESH,
+        )
+
+    loop(1, F, lambda d: greet((f + d) % F, t))
+    loop(1, T, lambda d: greet(f, (t + d) % T))
+
+    def greet_rows(k):
+        row = t * K + k
+
+        @pl.when(row != f)
+        def _():
+            loop(1, T, lambda d: greet(row, (t + d) % T))
+
+    loop(0, K, greet_rows)
+    loads[0].wait()
+    pl.semaphore_wait(barrier, F + T - 2 + (F - 1) * jnp.where(f // K == t, 0, 1))
+
     for o in range(1, T // 2):
         remote(tok, tk.at[t], s_tok.at[o], r_tok.at[t], f, (t + 2 * o) % T).start()
     remote(tok, tk.at[t], s_tok.at[T // 2], r_tok.at[t], f, t_pair).start()
     tk[t] = tok[...]
 
+    for load in loads[1:3]:
+        load.wait()
     experts = lax.broadcasted_iota(jnp.int32, (tok_count, E), 1)
     line = lax.broadcasted_iota(jnp.int32, (8, tok_count), 0)
     named_by = routes[...].astype(F32)
@@ -266,6 +323,8 @@
 
     loop(0, 1, direct_block)
 
+    for load in loads[3:6]:
+        load.wait()
     gains = jnp.broadcast_to(gain[...], (8, R)).T[:, 0:1]
 
     def fold(e):
@@ -281,6 +340,9 @@
         remote(gu_send.at[j], gu.at[f], s_gu.at[d], r_gu.at[f], j, t).start()
 
     loop(1, F, send_gu)
+
+    for load in loads[6:]:
+        load.wait()
 
     def fold_down(e):
         top, low = ed[e, : R // 2], ed[e, R // 2 :]
@@ -542,8 +604,14 @@
 
 
 def hand_on(count, *refs):
-    for i in range(count):
-        refs[count + i][...] = refs[i][...]
+    copies = [
+        pltpu.make_async_copy(refs[i], refs[count + i], refs[-1].at[i])
+        for i in range(count)
+    ]
+    for copy in copies:
+        copy.start()
+    for copy in copies:
+        copy.wait()
 
 
 def on_device(
@@ -567,6 +635,7 @@
     slots = (capacity + 15) // 16 * 16
     G, K = F // 2, F // T
     vmem = pl.BlockSpec(memory_space=pltpu.VMEM)
+    hbm = pl.BlockSpec(memory_space=pltpu.HBM)
     dma = pltpu.SemaphoreType.DMA
     shapes = [
         (tok_count, quarter),
@@ -600,16 +669,7 @@
         (T,), (T,), (F,), (F,), (F,), (K, T), (G,), (G,), (G,), (F,), (G,), (G,),
         (T // 2, F), (T // 2, F), (T, F), (T, G), (T, G), (G,), (G,), (G,), (E,), (T,), (T,),
     ]
-    results = pl.pallas_call(
-        functools.partial(kernel, F, T, slots),
-        out_shape=[jax.ShapeDtypeStruct(s, BF) for s in shapes],
-        in_specs=[vmem] * 10,
-        out_specs=[vmem] * 7,
-        scratch_shapes=[pltpu.VMEM(s, BF) for s in scratch] + [dma(s) for s in sems],
-        compiler_params=pltpu.CompilerParams(
-            has_side_effects=True, vmem_limit_bytes=60 * 1024 * 1024
-        ),
-    )(
+    args = (
         tokens,
         routes.T,
         route_weight.T,
@@ -621,11 +681,26 @@
         shared_up,
         shared_down,
     )
+    results = pl.pallas_call(
+        functools.partial(kernel, F, T, slots),
+        out_shape=[jax.ShapeDtypeStruct(s, BF) for s in shapes],
+        in_specs=[hbm] * 10,
+        out_specs=[vmem] * 7,
+        scratch_shapes=[pltpu.VMEM(a.shape, a.dtype) for a in args]
+        + [dma((len(args),))]
+        + [pltpu.VMEM(s, BF) for s in scratch]
+        + [dma(s) for s in sems],
+        compiler_params=pltpu.CompilerParams(
+            has_side_effects=True, collective_id=0, vmem_limit_bytes=24 * 1024 * 1024
+        ),
+    )(*[pltpu.with_memory_space_constraint(a, pltpu.HBM) for a in args])
     mixed, gate, up, down, sg, su, sd = pl.pallas_call(
         functools.partial(hand_on, 7),
         out_shape=[jax.ShapeDtypeStruct(s, BF) for s in shapes],
         in_specs=[vmem] * 7,
-        out_specs=[vmem] * 7,
+        out_specs=[hbm] * 7,
+        scratch_shapes=[dma((7,))],
+        compiler_params=pltpu.CompilerParams(vmem_limit_bytes=8 * 1024 * 1024),
     )(*results)
     return (mixed, gate.T[None], up.T[None], down[None], sg, su, sd)
 

time: 80.1 us -> 72.9 us (0.910)
  Pallas kernels: 79.3 us -> 72.1 us
    pallas_call x1, Pallas kernels: 76.2 us -> 70.6 us  [on_device(): pl.pallas_call(functools.partial(kernel, F, T, slots), out_shape=[jax.Sha...]
    pallas_call x1, Pallas kernels: 3.1 us -> 1.5 us  [on_device(): pl.pallas_call(functools.partial(hand_on, 7), out_shape=[jax.ShapeDtypeSt...]
where the time goes in v1:
time: 72.9 us; the launch traced here: 72.8 us
  Pallas kernels  72.1 us (99%)
    pallas_call x1, Pallas kernels, on_device(): pl.pallas_call(functools.partial(kernel, F, T, slots), out_shape=[jax.Sha...  70.6 us
    pallas_call x1, Pallas kernels, on_device(): pl.pallas_call(functools.partial(hand_on, 7), out_shape=[jax.ShapeDtypeSt...  1.5 us

profile of v1, /device:TPU:9, one launch (start us, length us, event | category | flops | bytes accessed | tf_op | source)
XLA Modules:
  0.0 72.8 jit_solution(16529640903252921703)
XLA Ops:
  0.6 70.6 %shard_map.153 = (bf16[128,512]{1,0:T(8,128)(2,1)S(1)}, bf16[64,2048]{1,0:T(8,128)(2,1)S(1)}, bf16[64,2048]{1,0:T(8,128)(2,1)S(1)}, bf16[512,256]{1,0:T(8,128)(2...) custom-call(bf16[128,512]{1,0:T(8,128)(2,1)} %tok_in.1, ...), custom_call_target="tpu_custom_call" | custom-call | tf_op jit(solution)/shard_map/pallas_call | solution.py:684
  71.3 1.5 %shard_map.154 = (bf16[128,512]{1,0:T(8,128)(2,1)}, bf16[64,2048]{1,0:T(8,128)(2,1)}, bf16[64,2048]{1,0:T(8,128)(2,1)}, bf16[512,256]{1,0:T(8,128)(2,1)}, bf16[2...) custom-call(bf16[128,512]{1,0:T(8,128)(2,1)S(1)} %get-tuple-element.21.refs_0_, ...), custom_call_target="tpu_custom_call" | custom-call | tf_op jit(solution)/shard_map/pallas_call | solution.py:697

commit v2 on v1

v2 whole, which is shorter than its diff:
```python
import functools

import jax
import jax.numpy as jnp
from jax import lax
from jax.experimental import pallas as pl
from jax.experimental.pallas import tpu as pltpu
from jax.sharding import PartitionSpec as P

EPS = 1e-06
BF = jnp.bfloat16
F32 = jnp.float32


def loop(low, high, body):
    def step(i, carry):
        body(i)
        return carry

    lax.fori_loop(low, high, step, 0)


def dot(a, b):
    return jnp.dot(a, b, preferred_element_type=F32)


def dot_nt(a, b):
    return lax.dot_general(a, b, (((1,), (1,)), ((), ())), preferred_element_type=F32)


def left_halves(a, b, half):
    lane = lax.broadcasted_iota(jnp.int32, a.shape, 1)
    return jnp.where(lane < half, a, pltpu.roll(b, half, 1))


def right_halves(a, b, half):
    lane = lax.broadcasted_iota(jnp.int32, a.shape, 1)
    return jnp.where(lane < half, pltpu.roll(a, half, 1), b)


def silu(v):
    return v / (1.0 + jnp.exp(-v))


def kernel(
    F,
    T,
    slots,
    tok_in,
    routes_in,
    weight_in,
    gain_in,
    eg_in,
    eu_in,
    ed_in,
    sg_in,
    su_in,
    sd_in,
    mixed,
    gate_out,
    up_out,
    dn_out,
    sg_out,
    su_out,
    sd_out,
    tok,
    routes,
    weight,
    gain,
    eg,
    eu,
    ed,
    sg,
    su,
    sd,
    s_load,
    tk,
    nm,
    gu_send,
    gu,
    dn_send,
    dn,
    sh,
    disp,
    port,
    hid,
    ret_send,
    ret,
    part,
    shr,
    s_tok,
    r_tok,
    s_gu,
    r_gu,
    f_gu,
    s_dn,
    r_dn,
    f_dn,
    s_left,
    s_right,
    s_shb,
    r_sh,
    s_da,
    p_out,
    p_in,
    r_port,
    s_out,
    s_in,
    r_hid,
    s_ret,
    r_ret,
    s_shr,
    r_shr,
):
    G = F // 2
    K = F // T
    H = T // 2
    E = eg.shape[0]
    R, C = eg.shape[1], eg.shape[2]
    half = C // 2
    tok_count = tok.shape[0]
    quarter = tok.shape[1]
    width = quarter * T
    f = lax.axis_index("fs")
    t = lax.axis_index("tp")
    g, p = f // 2, f % 2
    pair = g * 2 + (1 - p)
    y, c = t // 2, t % 2
    t_pair = y * 2 + (1 - c)
    home = f // K
    pieces = r_gu.shape[1]
    step = R // pieces
    mine = home == t

    def far_first(i):
        return jnp.where(2 * g < G, G - 1 - i, i)

    def near_first(i):
        return jnp.where(2 * g < G, i, G - 1 - i)

    def remote(src, dst, send, recv, fs, tp):
        return pltpu.make_async_remote_copy(
            src_ref=src,
            dst_ref=dst,
            send_sem=send,
            recv_sem=recv,
            device_id={"fs": fs, "tp": tp},
            device_id_type=pl.DeviceIdType.MESH,
        )

    def arrived(dst, send, recv):
        remote(dst, dst, send, recv, pair, t).wait_recv()

    def sent(src, send, recv):
        remote(src, src, send, recv, pair, t).wait_send()

    loads = [
        pltpu.make_async_copy(src, dst, s_load.at[i])
        for i, (src, dst) in enumerate(
            (
                (tok_in, tok),
                (routes_in, routes),
                (weight_in, weight),
                (gain_in, gain),
                (eg_in, eg),
                (eu_in, eu),
                (ed_in, ed),
                (sg_in, sg),
                (su_in, su),
                (sd_in, sd),
            )
        )
    ]
    for load in loads:
        load.start()

    barrier = pltpu.get_barrier_semaphore()

    def greet(fs, tp):
        pl.semaphore_signal(
            barrier,
            inc=1,
            device_id={"fs": fs, "tp": tp},
            device_id_type=pl.DeviceIdType.MESH,
        )

    loop(1, G, lambda d: greet(2 * ((g + d) % G) + p, t))
    greet(pair, t)
    loop(1, T, lambda d: greet(f, (t + d) % T))

    def greet_rows(i):
        row = t * K + 2 * i + p

        @pl.when(row != f)
        def _():
            loop(1, T, lambda d: greet(row, (t + d) % T))

    loop(0, K // 2, greet_rows)

    for load in loads[:3]:
        load.wait()
    experts = lax.broadcasted_iota(jnp.int32, (tok_count, E), 1)
    line = lax.broadcasted_iota(jnp.int32, (8, tok_count), 0)
    named_by = routes[...].astype(F32)
    turned = jnp.where(line == 0, named_by[0:1], named_by[1:2])
    turned = jnp.where(line == 2, weight[0:1, :], turned)
    turned = jnp.where(line == 3, weight[1:2, :], turned).T
    first, second = turned[:, 0:1].astype(jnp.int32), turned[:, 1:2].astype(jnp.int32)
    named = ((experts == first) | (experts == second)).astype(F32)
    rows = lax.broadcasted_iota(jnp.int32, (tok_count, tok_count), 0)
    cols = lax.broadcasted_iota(jnp.int32, (tok_count, tok_count), 1)
    before = (cols < rows).astype(F32).astype(BF)
    place = dot(before, named.astype(BF))
    slot_ids = lax.broadcasted_iota(jnp.int32, (tok_count, E * slots), 1)

    def spot_of(chosen):
        spot = jnp.sum(jnp.where(experts == chosen, place, 0.0), axis=1, keepdims=True)
        return spot.astype(jnp.int32)

    spot0, spot1 = spot_of(first), spot_of(second)
    pick0 = slot_ids == first * slots + spot0
    pick1 = slot_ids == second * slots + spot1
    both = jnp.where(pick0 | pick1, 1.0, 0.0).astype(BF)

    packed = lax.dot_general(
        both, tok[...], (((0,), (0,)), ((), ())), preferred_element_type=F32
    ).astype(BF)
    disp[...] = packed.reshape(E, slots, quarter)
    pl.semaphore_wait(barrier, G + T - 1 + (G - 1) * jnp.where(mine, 0, 1))

    def send_disp(i):
        e = far_first(i)

        @pl.when(e != g)
        def _():
            remote(
                disp.at[e], port.at[t, g], s_da.at[e], r_port.at[t, g], 2 * e + p, t
            ).start()

    loop(0, G, send_disp)
    port[t, g] = disp[g]

    def port_copy(src, group, sem, to):
        return remote(
            port.at[src, group], port.at[src, group], sem, r_port.at[src, group], f, to
        )

    def pass_block(group):
        for o in range(1, H):
            port_copy(t, group, p_out.at[o, group], (t + 2 * o) % T).start()
        port_copy(t, group, p_in.at[0, group], t_pair).start()

    pass_block(g)

    def tok_copy(src, sem, to):
        return remote(tk.at[src], tk.at[src], sem, r_tok.at[src], f, to)

    for o in range(1, H):
        remote(tok, tk.at[t], s_tok.at[o], r_tok.at[t], f, (t + 2 * o) % T).start()
    remote(tok, tk.at[t], s_tok.at[H], r_tok.at[t], f, t_pair).start()
    tk[t] = tok[...]

    def shared_copy(block, sems, to):
        return remote(sh.at[block], sh.at[block], sems, r_sh.at[block], to, t)

    def share_left(block):
        @pl.when(g > 0)
        def _():
            shared_copy(block, s_left.at[block // 2], f - 2).start()

    def share_right(block):
        @pl.when(g < G - 1)
        def _():
            shared_copy(block, s_right.at[block // 2], f + 2).start()

    def share_pair(block):
        shared_copy(block, s_shb.at[block // 2], pair).start()

    def relay_right(k):
        @pl.when(g - k >= 0)
        def _():
            block = f - 2 * k
            arrived(sh.at[block], s_right.at[0], r_sh.at[block])
            share_right(block)
            share_pair(block)

    def relay_left(k):
        @pl.when(g + k < G)
        def _():
            block = f + 2 * k
            arrived(sh.at[block], s_left.at[0], r_sh.at[block])
            share_left(block)
            share_pair(block)

    def relay_in(k):
        @pl.when(2 * g < G)
        def _():
            relay_right(k)

        @pl.when(2 * g >= G)
        def _():
            relay_left(k)

    def relay_out(k):
        @pl.when(2 * g < G)
        def _():
            relay_left(k)

        @pl.when(2 * g >= G)
        def _():
            relay_right(k)

    for load in loads[3:6]:
        load.wait()
    gains = jnp.broadcast_to(gain[...], (8, R)).T[:, 0:1]

    def rows_of(n):
        return pl.ds(pl.multiple_of(n * step, step), step)

    def send_gu(i):
        e = far_first(i)
        gu_send[e, :, :C] = (eg[e] * gains).astype(BF)
        gu_send[e, :, C:] = (eu[e] * gains).astype(BF)

        @pl.when(e != g)
        def _():
            def piece(n):
                remote(
                    gu_send.at[e, rows_of(n)],
                    gu.at[f, rows_of(n)],
                    s_gu.at[e, n],
                    r_gu.at[f, n],
                    2 * e + p,
                    t,
                ).start()

            loop(0, pieces, piece)

    loop(0, E, send_gu)
    gu[f] = gu_send[g]

    def cross(src, n):
        remote(
            gu.at[src, rows_of(n)],
            gu.at[src, rows_of(n)],
            f_gu.at[src // 2, n],
            r_gu.at[src, n],
            pair,
            t,
        ).start()

    loop(0, pieces, lambda n: cross(f, n))

    for load in loads[6:]:
        load.wait()
    sh[f, 0] = (sg[...] * gains).astype(BF)
    sh[f, 1] = (su[...] * gains).astype(BF)
    sh[f, 2] = sd[...].T.astype(BF)
    share_pair(f)

    def send_dn(i):
        e = far_first(i)
        dn_send[e] = ed[e].astype(BF)

        @pl.when(jnp.logical_not((e == g) & mine))
        def _():
            remote(
                dn_send.at[e], dn.at[f % K, t], s_dn.at[e], r_dn.at[f % K, t, 0], 2 * e + p, home
            ).start()

    loop(0, E, send_dn)

    @pl.when(mine)
    def _():
        dn[f % K, t] = dn_send[g]

    share_left(f)
    share_right(f)


    def take_block(i):
        group = near_first(i)

        @pl.when(group != g)
        def _():
            arrived(port.at[t, group], s_da.at[group], r_port.at[t, group])
            pass_block(group)

    loop(0, G, take_block)

    def inner_block(i):
        group = near_first(i)
        for o in range(1, H):
            src = (t + 2 * o) % T
            arrived(port.at[src, group], p_out.at[o, group], r_port.at[src, group])
            port_copy(src, group, p_in.at[o, group], t_pair).start()


    def take_near(i):
        src = 2 * jnp.where(2 * g < G, i, G - 1 - i) + p

        @pl.when(src != f)
        def _():
            def piece(n):
                arrived(gu.at[src, rows_of(n)], s_load.at[0], r_gu.at[src, n])
                cross(src, n)

            loop(0, pieces, piece)

    loop(0, G // 2, take_near)
    loop(0, G // 2, inner_block)

    def take_far(n):
        def block(i):
            src = 2 * jnp.where(2 * g < G, G // 2 + i, G // 2 - 1 - i) + p
            arrived(gu.at[src, rows_of(n)], s_load.at[0], r_gu.at[src, n])
            cross(src, n)

        loop(0, G // 2, block)

    loop(0, pieces // 2, take_far)
    loop(G // 2, G, inner_block)
    loop(pieces // 2, pieces, take_far)

    loop(1, G // 2, relay_in)

    for o in range(1, H):
        src = (t + 2 * o) % T
        arrived(tk.at[src], s_tok.at[o], r_tok.at[src])
        tok_copy(src, s_tok.at[H + o], t_pair).start()
    for o in range(H):
        src = (t_pair + 2 * o) % T
        arrived(tk.at[src], s_tok.at[o], r_tok.at[src])
    squares = jnp.zeros((tok_count, 1), F32)
    for q in range(T):
        x = tk[q].astype(F32)
        squares = squares + jnp.sum(x * x, axis=1, keepdims=True)
    scale = lax.rsqrt(squares / width + EPS)
    for q in range(T):
        nm[q] = (tk[q].astype(F32) * scale).astype(BF)
    def wait_inner(group):
        for o in range(H):
            src = (t_pair + 2 * o) % T
            arrived(port.at[src, group], p_in.at[o, group], r_port.at[src, group])

    loop(0, G, wait_inner)

    def crossed(i):
        src = 2 * near_first(i) + 1 - p
        loop(0, pieces, lambda n: arrived(gu.at[src, rows_of(n)], s_load.at[0], r_gu.at[src, n]))

    loop(0, G, crossed)

    def expert_hidden(i):
        group = far_first(i)
        total = jnp.zeros((slots, 2 * C), F32)
        squares = jnp.zeros((slots, 1), F32)
        for q in range(T):
            total = total + dot(
                port[q, group], gu[q * K : (q + 1) * K].reshape(quarter, 2 * C)
            )
            x = port[q, group].astype(F32)
            squares = squares + jnp.sum(x * x, axis=1, keepdims=True)
        total = total * lax.rsqrt(squares / width + EPS)
        hid[t, group] = (silu(total[:, :C]) * total[:, C:]).astype(BF)
        for o in range(1, H):
            remote(
                hid.at[t, group],
                hid.at[t, group],
                s_out.at[o, group],
                r_hid.at[t, group],
                f,
                (t + 2 * o) % T,
            ).start()
        remote(
            hid.at[t, group],
            hid.at[t, group],
            s_in.at[0, group],
            r_hid.at[t, group],
            f,
            t_pair,
        ).start()

    loop(0, G, expert_hidden)

    def hand_across(i, ref, recv, hand):
        k = 2 * i + p
        count = recv.shape[2]
        rows = R // count

        def piece(n):
            span = pl.ds(pl.multiple_of(n * rows, rows), rows)

            def chunk(q):
                part_of = ref.at[k, q, span]

                @pl.when(jnp.logical_not((t * K + k == f) & (q == t)))
                def _():
                    arrived(part_of, s_load.at[0], recv.at[k, q, n])

                remote(
                    part_of, part_of, hand.at[i, q, n], recv.at[k, q, n], pair, t
                ).start()

            loop(0, T, chunk)

        loop(0, count, piece)

    def handed(i, ref, recv):
        k = 2 * i + 1 - p
        count = recv.shape[2]
        rows = R // count

        def piece(n):
            span = pl.ds(pl.multiple_of(n * rows, rows), rows)
            loop(0, T, lambda q: arrived(ref.at[k, q, span], s_load.at[0], recv.at[k, q, n]))

        loop(0, count, piece)

    loop(0, K // 2, lambda i: hand_across(i, dn, r_dn, f_dn))
    loop(1, G // 2 + 1, relay_out)

    def pass_hidden(i):
        group = far_first(i)
        for o in range(1, H):
            src = (t + 2 * o) % T
            arrived(hid.at[src, group], s_out.at[o, group], r_hid.at[src, group])
            remote(
                hid.at[src, group],
                hid.at[src, group],
                s_in.at[o, group],
                r_hid.at[src, group],
                f,
                t_pair,
            ).start()

    loop(0, G, pass_hidden)
    loop(0, K // 2, lambda i: handed(i, dn, r_dn))

    def expert_out(i):
        group = far_first(i)
        for o in range(H):
            src = (t_pair + 2 * o) % T
            arrived(hid.at[src, group], s_in.at[o, group], r_hid.at[src, group])
        total = jnp.zeros((slots, quarter), F32)
        for q in range(T):
            total = total + dot_nt(hid[q, group], dn[:, q].reshape(K * R, C))
        ret_send[group] = total.astype(BF)

        @pl.when(group != g)
        def _():
            remote(
                ret_send.at[group], ret.at[g], s_ret.at[group], r_ret.at[g], 2 * group + p, t
            ).start()

    loop(0, G, expert_out)
    ret[g] = ret_send[g]

    loop(G // 2 + 1, G, relay_out)
    loop(G // 2, G, relay_in)

    def place_down(k):
        for q in range(0, T, 2):
            a, b = dn[k, q].astype(F32), dn[k, q + 1].astype(F32)
            block = jnp.where(
                p == 0, left_halves(a, b, half), right_halves(a, b, half)
            )
            dn_out[pl.ds(pl.multiple_of(k * R, R), R), q * half : (q + 2) * half] = block.astype(BF)

    loop(0, K, place_down)

    def wait_shared(d):
        block = ((g + G - d) % G) * 2 + 1 - p
        arrived(sh.at[block], s_shb.at[d], r_sh.at[block])

    loop(0, G, wait_shared)

    gate_sh = sh[:, 0].reshape(F * R, C)
    up_sh = sh[:, 1].reshape(F * R, C)
    down_sh = sh[:, 2].reshape(F * R, C)
    act = jnp.zeros((tok_count, C), F32)
    lin = jnp.zeros((tok_count, C), F32)
    for q in range(T):
        act = act + dot(nm[q], gate_sh[q * quarter : (q + 1) * quarter])
        lin = lin + dot(nm[q], up_sh[q * quarter : (q + 1) * quarter])
    hidden_sh = (silu(act) * lin).astype(BF)
    for q in range(T):
        part[q] = dot_nt(hidden_sh, down_sh[q * quarter : (q + 1) * quarter]).astype(BF)
    shr[t] = part[t]

    def send_part(d):
        q = (t + d) % T
        remote(part.at[q], shr.at[t], s_shr.at[d], r_shr.at[t], f, q).start()

    loop(1, T, send_part)

    for q in range(T):
        span = slice(q * quarter, (q + 1) * quarter)
        sd_out[:, span] = (
            sh[q * K : (q + 1) * K, 2].reshape(quarter, C).astype(F32).T.astype(BF)
        )
    sg_out[...] = sh[:, 0].reshape(F * R, C)
    su_out[...] = sh[:, 1].reshape(F * R, C)

    for q in range(T):
        span = slice(q * quarter, (q + 1) * quarter)
        whole = gu[q * K : (q + 1) * K].reshape(quarter, 2 * C).astype(F32)
        gate, up = whole[:, :C].T, whole[:, C:].T
        gate_out[:, span] = jnp.where(p == 0, gate[:half], gate[half:]).astype(BF)
        up_out[:, span] = jnp.where(p == 0, up[:half], up[half:]).astype(BF)

    def wait_ret(d):
        src = (g + d) % G
        arrived(ret.at[src], s_ret.at[src], r_ret.at[src])

    loop(1, G, wait_ret)
    outs = ret[...].reshape(E * slots, quarter)
    routed = jnp.zeros((tok_count, quarter), F32)
    for k, pick in enumerate((pick0, pick1)):
        chosen = jnp.where(pick, 1.0, 0.0).astype(BF)
        routed = routed + turned[:, 2 + k : 3 + k] * dot(chosen, outs)

    def wait_part(d):
        src = (t + d) % T
        arrived(shr.at[src], s_shr.at[d], r_shr.at[src])

    loop(1, T, wait_part)
    total = shr[0].astype(F32)
    for q in range(1, T):
        total = total + shr[q].astype(F32)
    mixed[...] = (total + routed).astype(BF)

    def done_tp(d):
        sent(tok, s_tok.at[d], r_tok.at[0])
        sent(part.at[0], s_shr.at[d], r_shr.at[0])

    loop(1, T, done_tp)

    def done_experts(e):
        @pl.when(jnp.logical_not((e == g) & mine))
        def _():
            sent(dn_send.at[0], s_dn.at[e], r_dn.at[0, 0, 0])

        @pl.when(e != g)
        def _():
            loop(0, pieces, lambda n: sent(gu_send.at[0, :step], s_gu.at[e, n], r_gu.at[0, 0]))
            sent(disp.at[0], s_da.at[e], r_port.at[0, 0])
            sent(ret_send.at[0], s_ret.at[e], r_ret.at[0])

        loop(0, pieces, lambda n: sent(gu.at[0, :step], f_gu.at[e, n], r_gu.at[0, 0]))
        for o in range(1, H):
            sent(disp.at[0], p_out.at[o, e], r_port.at[0, 0])
            sent(hid.at[0, 0], s_out.at[o, e], r_hid.at[0, 0])
        for o in range(H):
            sent(disp.at[0], p_in.at[o, e], r_port.at[0, 0])
            sent(hid.at[0, 0], s_in.at[o, e], r_hid.at[0, 0])

    loop(0, G, done_experts)

    def done_hands(i):
        def chunk(q):
            sent(dn.at[0, 0], f_dn.at[i, q, 0], r_dn.at[0, 0, 0])

        loop(0, T, chunk)

    loop(0, K // 2, done_hands)

    def done_groups(d):
        sent(sh.at[f], s_shb.at[d], r_sh.at[0])

        @pl.when((d >= g) & (g > 0))
        def _():
            sent(sh.at[f], s_left.at[d], r_sh.at[0])

        @pl.when((d <= g) & (g < G - 1))
        def _():
            sent(sh.at[f], s_right.at[d], r_sh.at[0])

    loop(0, G, done_groups)


def hand_on(count, *refs):
    copies = [
        pltpu.make_async_copy(refs[i], refs[count + i], refs[-1].at[i])
        for i in range(count)
    ]
    for copy in copies:
        copy.start()
    for copy in copies:
        copy.wait()


def on_device(
    tokens,
    routes,
    route_weight,
    norm_gain,
    expert_gate,
    expert_up,
    expert_down,
    shared_gate,
    shared_up,
    shared_down,
):
    F = lax.axis_size("fs")
    T = lax.axis_size("tp")
    E, R, C = expert_gate.shape
    tok_count, quarter = tokens.shape
    pick_count = routes.shape[1]
    capacity = 2 * ((3 * tok_count * pick_count + 4 * E - 1) // (4 * E))
    slots = (capacity + 15) // 16 * 16
    G, K = F // 2, F // T
    vmem = pl.BlockSpec(memory_space=pltpu.VMEM)
    hbm = pl.BlockSpec(memory_space=pltpu.HBM)
    dma = pltpu.SemaphoreType.DMA
    shapes = [
        (tok_count, quarter),
        (C // 2, F * R),
        (C // 2, F * R),
        (K * R, T * C // 2),
        (F * R, C),
        (F * R, C),
        (C, F * R),
    ]
    H, N = T // 2, max(R // 64, 1)
    scratch = [
        (T, tok_count, quarter),
        (T, tok_count, quarter),
        (E, R, 2 * C),
        (F, R, 2 * C),
        (E, R, C),
        (K, T, R, C),
        (F, 3, R, C),
        (E, slots, quarter),
        (T, G, slots, quarter),
        (T, G, slots, C),
        (G, slots, quarter),
        (G, slots, quarter),
        (T, tok_count, quarter),
        (T, tok_count, quarter),
    ]
    sems = [
        (T,), (T,), (E, N), (F, N), (G, N), (E,), (K, T, 1), (K // 2, T, 1),
        (G,), (G,), (G,), (F,), (E,), (H, G), (H, G), (T, G),
        (H, G), (H, G), (T, G), (G,), (G,), (T,), (T,),
    ]
    args = (
        tokens,
        routes.T,
        route_weight.T,
        norm_gain[None, :],
        expert_gate,
        expert_up,
        expert_down,
        shared_gate,
        shared_up,
        shared_down,
    )
    results = pl.pallas_call(
        functools.partial(kernel, F, T, slots),
        out_shape=[jax.ShapeDtypeStruct(s, BF) for s in shapes],
        in_specs=[hbm] * 10,
        out_specs=[vmem] * 7,
        scratch_shapes=[pltpu.VMEM(a.shape, a.dtype) for a in args]
        + [dma((len(args),))]
        + [pltpu.VMEM(s, BF) for s in scratch]
        + [dma(s) for s in sems],
        compiler_params=pltpu.CompilerParams(
            has_side_effects=True, collective_id=0, vmem_limit_bytes=32 * 1024 * 1024
        ),
    )(*[pltpu.with_memory_space_constraint(a, pltpu.HBM) for a in args])
    mixed, gate, up, down, sg, su, sd = pl.pallas_call(
        functools.partial(hand_on, 7),
        out_shape=[jax.ShapeDtypeStruct(s, BF) for s in shapes],
        in_specs=[vmem] * 7,
        out_specs=[hbm] * 7,
        scratch_shapes=[dma((7,))],
        compiler_params=pltpu.CompilerParams(vmem_limit_bytes=8 * 1024 * 1024),
    )(*results)
    return (mixed, gate.T[None], up.T[None], down[None], sg, su, sd)


def solution(mesh):
    in_specs = (
        P("fs", "tp"),
        P("fs", None),
        P("fs", None),
        P("fs"),
        P(None, "fs", "tp"),
        P(None, "fs", "tp"),
        P(None, "fs", "tp"),
        P("fs", "tp"),
        P("fs", "tp"),
        P("tp", "fs"),
    )
    out_specs = (
        P("fs", "tp"),
        P("fs", None, "tp"),
        P("fs", None, "tp"),
        P("fs", "tp", None),
        P(None, "tp"),
        P(None, "tp"),
        P("tp", None),
    )
    return jax.shard_map(
        on_device, mesh=mesh, in_specs=in_specs, out_specs=out_specs, check_vma=False
    )
```

time: 72.9 us -> 66.2 us (0.908)
  the two profiles are of different devices: /device:TPU:9 before, /device:TPU:0 now
where the time goes in v2:
time: 66.2 us; the launch traced here: 66.1 us
  Pallas kernels  65.4 us (99%)
    pallas_call x1, Pallas kernels, on_device(): pl.pallas_call(functools.partial(kernel, F, T, slots), out_shape=[jax.Sha...  63.9 us
    pallas_call x1, Pallas kernels, on_device(): pl.pallas_call(functools.partial(hand_on, 7), out_shape=[jax.ShapeDtypeSt...  1.5 us

profile of v2, /device:TPU:0, one launch (start us, length us, event | category | flops | bytes accessed | tf_op | source)
XLA Modules:
  0.0 66.1 jit_solution(3176895011367811262)
XLA Ops:
  0.6 63.9 %shard_map.153 = (bf16[128,512]{1,0:T(8,128)(2,1)S(1)}, bf16[64,2048]{1,0:T(8,128)(2,1)S(1)}, bf16[64,2048]{1,0:T(8,128)(2,1)S(1)}, bf16[512,256]{1,0:T(8,128)(2...) custom-call(bf16[128,512]{1,0:T(8,128)(2,1)} %tok_in.1, ...), custom_call_target="tpu_custom_call" | custom-call | tf_op jit(solution)/shard_map/pallas_call | solution.py:759
  64.6 1.5 %shard_map.154 = (bf16[128,512]{1,0:T(8,128)(2,1)}, bf16[64,2048]{1,0:T(8,128)(2,1)}, bf16[64,2048]{1,0:T(8,128)(2,1)}, bf16[512,256]{1,0:T(8,128)(2,1)}, bf16[2...) custom-call(bf16[128,512]{1,0:T(8,128)(2,1)S(1)} %get-tuple-element.21.refs_0_, ...), custom_call_target="tpu_custom_call" | custom-call | tf_op jit(solution)/shard_map/pallas_call | solution.py:772

commit v3 on v2

v3 whole, which is shorter than its diff:
```python
import functools

import jax
import jax.numpy as jnp
from jax import lax
from jax.experimental import pallas as pl
from jax.experimental.pallas import tpu as pltpu
from jax.sharding import PartitionSpec as P

EPS = 1e-06
BF = jnp.bfloat16
F32 = jnp.float32


def loop(low, high, body):
    def step(i, carry):
        body(i)
        return carry

    lax.fori_loop(low, high, step, 0)


def dot(a, b):
    return jnp.dot(a, b, preferred_element_type=F32)


def dot_nt(a, b):
    return lax.dot_general(a, b, (((1,), (1,)), ((), ())), preferred_element_type=F32)


def left_halves(a, b, half):
    lane = lax.broadcasted_iota(jnp.int32, a.shape, 1)
    return jnp.where(lane < half, a, pltpu.roll(b, half, 1))


def right_halves(a, b, half):
    lane = lax.broadcasted_iota(jnp.int32, a.shape, 1)
    return jnp.where(lane < half, pltpu.roll(a, half, 1), b)


def silu(v):
    return v / (1.0 + jnp.exp(-v))


def kernel(
    F,
    T,
    slots,
    tok_in,
    routes_in,
    weight_in,
    gain_in,
    eg_in,
    eu_in,
    ed_in,
    sg_in,
    su_in,
    sd_in,
    mixed,
    gate_out,
    up_out,
    dn_out,
    sg_out,
    su_out,
    sd_out,
    tok,
    routes,
    weight,
    gain,
    eg,
    eu,
    ed,
    sg,
    su,
    sd,
    s_load,
    tk,
    nm,
    gu_send,
    gu,
    dn_send,
    dn,
    sh,
    disp,
    port,
    hid,
    ret_send,
    ret,
    hsh,
    sdx,
    raw,
    gw_send,
    meta_send,
    meta,
    s_tok,
    r_tok,
    s_gu,
    r_gu,
    x_gu,
    f_gu,
    s_dn,
    r_dn,
    x_dn,
    f_dn,
    s_left,
    s_right,
    s_shb,
    r_sh,
    r_shp,
    s_da,
    p_out,
    p_in,
    r_port,
    x_port,
    s_raw,
    r_raw,
    s_meta,
    r_meta,
    s_gw,
    s_out,
    s_in,
    r_hid,
    s_ret,
    r_ret,
    s_hsh,
    r_hsh,
    s_sdx,
    r_sdx,
):
    G = F // 2
    K = F // T
    H = T // 2
    E = eg.shape[0]
    R, C = eg.shape[1], eg.shape[2]
    half = C // 2
    tok_count = tok.shape[0]
    quarter = tok.shape[1]
    width = quarter * T
    f = lax.axis_index("fs")
    t = lax.axis_index("tp")
    g, p = f // 2, f % 2
    pair = g * 2 + (1 - p)
    y, c = t // 2, t % 2
    t_pair = y * 2 + (1 - c)
    home = f // K
    pieces = r_gu.shape[1]
    D = G // 2
    step = R // pieces
    mine = home == t

    def far_first(i):
        return jnp.where(2 * g < G, G - 1 - i, i)

    def near_first(i):
        return jnp.where(2 * g < G, i, G - 1 - i)

    def send_order(i):
        return jnp.where(i < G // 2, near_first(i), far_first(i - G // 2))

    left = 2 * g < G
    depth = jnp.where(left, g, G - 1 - g)
    gateway = jnp.where(left, D, D - 1)

    def remote(src, dst, send, recv, fs, tp):
        return pltpu.make_async_remote_copy(
            src_ref=src,
            dst_ref=dst,
            send_sem=send,
            recv_sem=recv,
            device_id={"fs": fs, "tp": tp},
            device_id_type=pl.DeviceIdType.MESH,
        )

    def arrived(dst, send, recv):
        remote(dst, dst, send, recv, pair, t).wait_recv()

    def sent(src, send, recv):
        remote(src, src, send, recv, pair, t).wait_send()

    loads = [
        pltpu.make_async_copy(src, dst, s_load.at[i])
        for i, (src, dst) in enumerate(
            (
                (tok_in, tok),
                (routes_in, routes),
                (weight_in, weight),
                (gain_in, gain),
                (eg_in, eg),
                (eu_in, eu),
                (ed_in, ed),
                (sg_in, sg),
                (su_in, su),
                (sd_in, sd),
            )
        )
    ]
    for load in loads:
        load.start()

    barrier = pltpu.get_barrier_semaphore()

    def greet(fs, tp):
        pl.semaphore_signal(
            barrier,
            inc=1,
            device_id={"fs": fs, "tp": tp},
            device_id_type=pl.DeviceIdType.MESH,
        )

    loop(1, G, lambda d: greet(2 * ((g + d) % G) + p, t))
    greet(pair, t)
    loop(1, T, lambda d: greet(f, (t + d) % T))

    def greet_rows(i):
        row = t * K + 2 * i + p

        @pl.when(row != f)
        def _():
            loop(1, T, lambda d: greet(row, (t + d) % T))

    loop(0, K // 2, greet_rows)

    for load in loads[:2]:
        load.wait()
    named_by = routes[...].astype(F32)
    line = lax.broadcasted_iota(jnp.int32, (8, tok_count), 0)
    meta_send[...] = jnp.where(line == 0, named_by[0:1], named_by[1:2])
    rows = lax.broadcasted_iota(jnp.int32, (tok_count, tok_count), 0)
    cols = lax.broadcasted_iota(jnp.int32, (tok_count, tok_count), 1)
    after = (rows < cols).astype(F32).astype(BF)
    slot_rows = lax.broadcasted_iota(jnp.int32, (slots, tok_count), 0)

    def pack(e, names, block):
        chosen = e.astype(F32)
        held = ((names[0:1] == chosen) | (names[1:2] == chosen)).astype(F32)
        spots = dot(jnp.broadcast_to(held, (16, tok_count)).astype(BF), after)
        here = (slot_rows == spots[0:1].astype(jnp.int32)) & (held > 0.5)
        return dot(here.astype(F32).astype(BF), block).astype(BF)

    def at_depth(i):
        return jnp.where(left, i, G - 1 - i)

    for i in range(D):
        disp[i] = pack(at_depth(i), meta_send[...], tok[...])
    pl.semaphore_wait(barrier, G + T - 1 + (G - 1) * jnp.where(mine, 0, 1))
    remote(tok, raw.at[depth], s_raw.at[0], r_raw.at[depth], 2 * gateway + p, t).start()
    remote(
        meta_send, meta.at[depth], s_meta.at[0], r_meta.at[depth], 2 * gateway + p, t
    ).start()

    def send_disp(i):
        @pl.when(i != depth)
        def _():
            remote(
                disp.at[i],
                port.at[t, g],
                s_da.at[0],
                r_port.at[0, g],
                2 * at_depth(i) + p,
                t,
            ).start()

    loop(0, D, send_disp)
    port[t, g] = disp[depth]

    def port_copy(src, group, sem, recv, to):
        return remote(port.at[src, group], port.at[src, group], sem, recv, f, to)

    def pass_block(group):
        for o in range(1, H):
            port_copy(
                t, group, p_out.at[0], r_port.at[H - o, group], (t + 2 * o) % T
            ).start()
        port_copy(t, group, p_in.at[0], x_port.at[0], t_pair).start()

    pass_block(g)

    def tok_copy(src, sem, to):
        return remote(tk.at[src], tk.at[src], sem, r_tok.at[src], f, to)

    for o in range(1, H):
        remote(tok, tk.at[t], s_tok.at[0], r_tok.at[t], f, (t + 2 * o) % T).start()
    remote(tok, tk.at[t], s_tok.at[0], r_tok.at[t], f, t_pair).start()
    tk[t] = tok[...]

    def shared_copy(block, i, sems, recv, to):
        return remote(sh.at[block, i], sh.at[block, i], sems, recv, to, t)

    def share_left(block, i):
        @pl.when(g > 0)
        def _():
            shared_copy(block, i, s_left.at[block // 2], r_sh.at[block // 2, i], f - 2).start()

    def share_right(block, i):
        @pl.when(g < G - 1)
        def _():
            shared_copy(block, i, s_right.at[block // 2], r_sh.at[block // 2, i], f + 2).start()

    def share_pair(block, i):
        shared_copy(block, i, s_shb.at[0], r_shp.at[block // 2, (i + 1) // 2], pair).start()

    def spread(block):
        @pl.when(block // K != t)
        def _():
            remote(
                sh.at[block, 0],
                sdx.at[t, block % K],
                s_sdx.at[0],
                r_sdx.at[0],
                f,
                block // K,
            ).start()

    def relay_right(k):
        @pl.when(g - k >= 0)
        def _():
            block = f - 2 * k

            def piece(i):
                arrived(sh.at[block, i], s_load.at[0], r_sh.at[block // 2, i])
                share_right(block, i)
                share_pair(block, i)

            loop(0, 3, piece)
            spread(block)

    def relay_left(k):
        @pl.when(g + k < G)
        def _():
            block = f + 2 * k

            def piece(i):
                arrived(sh.at[block, i], s_load.at[0], r_sh.at[block // 2, i])
                share_left(block, i)
                share_pair(block, i)

            loop(0, 3, piece)
            spread(block)

    def relay_in(k):
        @pl.when(2 * g < G)
        def _():
            relay_right(k)

        @pl.when(2 * g >= G)
        def _():
            relay_left(k)

    def relay_out(k):
        @pl.when(2 * g < G)
        def _():
            relay_left(k)

        @pl.when(2 * g >= G)
        def _():
            relay_right(k)

    for load in loads[2:6]:
        load.wait()
    gains = jnp.broadcast_to(gain[...], (8, R)).T[:, 0:1]

    def rows_of(n):
        return pl.ds(pl.multiple_of(n * step, step), step)

    def send_gu(i):
        e = send_order(i)
        gu_send[e, :, :C] = (eg[e] * gains).astype(BF)
        gu_send[e, :, C:] = (eu[e] * gains).astype(BF)

        @pl.when(e != g)
        def _():
            def piece(n):
                remote(
                    gu_send.at[e, rows_of(n)],
                    gu.at[f, rows_of(n)],
                    s_gu.at[0],
                    r_gu.at[g, n],
                    2 * e + p,
                    t,
                ).start()

            loop(0, pieces, piece)

    loop(0, E, send_gu)
    gu[f] = gu_send[g]

    def cross(src, n):
        remote(
            gu.at[src, rows_of(n)],
            gu.at[src, rows_of(n)],
            f_gu.at[0],
            x_gu.at[0],
            pair,
            t,
        ).start()

    loop(0, pieces, lambda n: cross(f, n))

    for load in loads[6:]:
        load.wait()
    sh[f, 0] = sd[...].T.astype(BF)
    sh[f, 1] = (sg[...] * gains).astype(BF)
    sh[f, 2] = (su[...] * gains).astype(BF)
    spread(f)
    loop(0, 3, lambda i: share_pair(f, i))

    def take_block(group):
        arrived(port.at[t, group], s_load.at[0], r_port.at[0, group])
        pass_block(group)

    def take_side(i):
        @pl.when(i != depth)
        def _():
            take_block(at_depth(i))

    def take_other(i):
        take_block(at_depth(G - 1 - i))

    def open_block(i):
        group = at_depth(G - 1 - i)
        arrived(raw.at[i], s_load.at[0], r_raw.at[i])
        arrived(meta.at[i], s_load.at[0], r_meta.at[i])
        for k in range(D - 1):
            gw_send[i, k] = pack(at_depth(k), meta[i], raw[i])
            remote(
                gw_send.at[i, k],
                port.at[t, group],
                s_gw.at[0],
                r_port.at[0, group],
                2 * at_depth(k) + p,
                t,
            ).start()
        port[t, group] = pack(g, meta[i], raw[i])
        pass_block(group)

    def inner_block(i):
        group = near_first(i)
        for o in range(1, H):
            src = (t + 2 * o) % T
            arrived(port.at[src, group], s_load.at[0], r_port.at[o, group])
            port_copy(src, group, p_in.at[0], x_port.at[0], t_pair).start()


    def take_near(i):
        src = 2 * jnp.where(2 * g < G, i, G - 1 - i) + p

        @pl.when(src != f)
        def _():
            def piece(n):
                arrived(gu.at[src, rows_of(n)], s_load.at[0], r_gu.at[src // 2, n])
                cross(src, n)

            loop(0, pieces, piece)


    def take_far(n):
        def block(i):
            src = 2 * jnp.where(2 * g < G, G // 2 + i, G // 2 - 1 - i) + p
            arrived(gu.at[src, rows_of(n)], s_load.at[0], r_gu.at[src // 2, n])
            cross(src, n)

        loop(0, G // 2, block)


    def expert_hidden(i):
        group = near_first(i)
        total = jnp.zeros((slots, 2 * C), F32)
        squares = jnp.zeros((slots, 1), F32)
        for q in range(T):
            total = total + dot(
                port[q, group], gu[q * K : (q + 1) * K].reshape(quarter, 2 * C)
            )
            x = port[q, group].astype(F32)
            squares = squares + jnp.sum(x * x, axis=1, keepdims=True)
        total = total * lax.rsqrt(squares / width + EPS)
        hid[t, group] = (silu(total[:, :C]) * total[:, C:]).astype(BF)
        for o in range(1, H):
            remote(
                hid.at[t, group],
                hid.at[t, group],
                s_out.at[0],
                r_hid.at[H - o, group],
                f,
                (t + 2 * o) % T,
            ).start()
        remote(
            hid.at[t, group],
            hid.at[t, group],
            s_in.at[0],
            r_hid.at[0, group],
            f,
            t_pair,
        ).start()


    def hand_across(i):
        k = 2 * i + p

        def chunk(q):
            @pl.when(jnp.logical_not((t * K + k == f) & (q == t)))
            def _():
                arrived(dn.at[k, q], s_load.at[0], r_dn.at[i, q])

            remote(dn.at[k, q], dn.at[k, q], f_dn.at[0], x_dn.at[0], pair, t).start()

        loop(0, T, chunk)

    def pass_hidden(i):
        group = near_first(i)
        for o in range(1, H):
            src = (t + 2 * o) % T
            arrived(hid.at[src, group], s_load.at[0], r_hid.at[o, group])
            remote(
                hid.at[src, group],
                hid.at[src, group],
                s_in.at[0],
                r_hid.at[0, group],
                f,
                t_pair,
            ).start()


    def expert_out(i):
        group = near_first(i)
        arrived(hid.at[:H, group], s_load.at[0], r_hid.at[0, group])
        total = jnp.zeros((slots, quarter), F32)
        for q in range(T):
            total = total + dot_nt(hid[q, group], dn[:, q].reshape(K * R, C))
        ret_send[group] = total.astype(BF)

        @pl.when(group != g)
        def _():
            remote(
                ret_send.at[group], ret.at[g], s_ret.at[0], r_ret.at[0], 2 * group + p, t
            ).start()


    at_gate = depth == D - 1

    @pl.when(at_gate)
    def _():
        loop(0, D, lambda i: open_block(D - 1 - i))

    loop(0, D, take_side)

    def send_dn(i):
        e = send_order(i)
        dn_send[e] = ed[e].astype(BF)

        @pl.when(jnp.logical_not((e == g) & mine))
        def _():
            remote(
                dn_send.at[e], dn.at[f % K, t], s_dn.at[0], r_dn.at[f % K // 2, t], 2 * e + p, home
            ).start()

    loop(0, E, send_dn)

    @pl.when(mine)
    def _():
        dn[f % K, t] = dn_send[g]

    loop(0, 3, lambda i: share_left(f, i))
    loop(0, 3, lambda i: share_right(f, i))


    loop(0, G // 2, take_near)

    @pl.when(jnp.logical_not(at_gate))
    def _():
        loop(0, D, lambda i: take_other(D - 1 - i))

    loop(0, pieces, take_far)
    loop(0, G, inner_block)
    loop(0, K // 2, hand_across)
    loop(1, G // 2, relay_in)

    for o in range(1, H):
        src = (t + 2 * o) % T
        arrived(tk.at[src], s_load.at[0], r_tok.at[src])
        tok_copy(src, s_tok.at[0], t_pair).start()
    for o in range(H):
        src = (t_pair + 2 * o) % T
        arrived(tk.at[src], s_load.at[0], r_tok.at[src])
    squares = jnp.zeros((tok_count, 1), F32)
    for q in range(T):
        x = tk[q].astype(F32)
        squares = squares + jnp.sum(x * x, axis=1, keepdims=True)
    scale = lax.rsqrt(squares / width + EPS)
    for q in range(T):
        nm[q] = (tk[q].astype(F32) * scale).astype(BF)
    arrived(port.at[:H], s_load.at[0], x_port.at[0])
    arrived(gu.at[:G], s_load.at[0], x_gu.at[0])
    loop(0, G, expert_hidden)
    loop(1, min(2, G), relay_out)
    loop(0, G, pass_hidden)
    at_end = (g == 0) | (g == G - 1)

    @pl.when(jnp.logical_not(at_end))
    def _():
        loop(2, G // 2 + 1, relay_out)

    arrived(dn.at[: K // 2], s_load.at[0], x_dn.at[0])
    loop(0, G, expert_out)
    ret[g] = ret_send[g]

    @pl.when(at_end)
    def _():
        loop(2, G // 2 + 1, relay_out)

    loop(G // 2 + 1, G, relay_out)
    loop(G // 2, G, relay_in)

    def place_down(k):
        for q in range(0, T, 2):
            a, b = dn[k, q].astype(F32), dn[k, q + 1].astype(F32)
            block = jnp.where(
                p == 0, left_halves(a, b, half), right_halves(a, b, half)
            )
            dn_out[pl.ds(pl.multiple_of(k * R, R), R), q * half : (q + 2) * half] = block.astype(BF)

    loop(0, K, place_down)

    def wait_down(i):
        block = near_first(i) * 2 + 1 - p
        arrived(sh.at[block, 0], s_load.at[0], r_shp.at[block // 2, 0])
        spread(block)
        arrived(sh.at[block, 1:3], s_load.at[0], r_shp.at[block // 2, 1])

    loop(0, G, wait_down)

    gate_sh = sh[:, 1].reshape(F * R, C)
    up_sh = sh[:, 2].reshape(F * R, C)
    act = jnp.zeros((tok_count, C), F32)
    lin = jnp.zeros((tok_count, C), F32)
    for q in range(T):
        act = act + dot(nm[q], gate_sh[q * quarter : (q + 1) * quarter])
        lin = lin + dot(nm[q], up_sh[q * quarter : (q + 1) * quarter])
    hsh[t] = (silu(act) * lin).astype(BF)

    def send_hsh(d):
        remote(
            hsh.at[t], hsh.at[t], s_hsh.at[0], r_hsh.at[0], f, (t + d) % T
        ).start()

    loop(1, T, send_hsh)

    def keep_down(k):
        sdx[t, k] = sh[t * K + k, 0]

    loop(0, K, keep_down)

    for q in range(T):
        span = slice(q * quarter, (q + 1) * quarter)
        sd_out[:, span] = (
            sh[q * K : (q + 1) * K, 0].reshape(quarter, C).astype(F32).T.astype(BF)
        )
    sg_out[...] = sh[:, 1].reshape(F * R, C)
    su_out[...] = sh[:, 2].reshape(F * R, C)

    for q in range(T):
        span = slice(q * quarter, (q + 1) * quarter)
        whole = gu[q * K : (q + 1) * K].reshape(quarter, 2 * C).astype(F32)
        gate, up = whole[:, :C].T, whole[:, C:].T
        gate_out[:, span] = jnp.where(p == 0, gate[:half], gate[half:]).astype(BF)
        up_out[:, span] = jnp.where(p == 0, up[:half], up[half:]).astype(BF)

    experts = lax.broadcasted_iota(jnp.int32, (tok_count, E), 1)
    turned = jnp.where(line == 2, weight[0:1, :], meta_send[...])
    turned = jnp.where(line == 3, weight[1:2, :], turned).T
    first, second = turned[:, 0:1].astype(jnp.int32), turned[:, 1:2].astype(jnp.int32)
    named = ((experts == first) | (experts == second)).astype(F32)
    before = (cols < rows).astype(F32).astype(BF)
    place = dot(before, named.astype(BF))
    slot_ids = lax.broadcasted_iota(jnp.int32, (tok_count, E * slots), 1)

    def pick_of(chosen):
        spot = jnp.sum(jnp.where(experts == chosen, place, 0.0), axis=1, keepdims=True)
        return slot_ids == chosen * slots + spot.astype(jnp.int32)

    pick0, pick1 = pick_of(first), pick_of(second)

    arrived(ret.at[: G - 1], s_load.at[0], r_ret.at[0])
    outs = ret[...].reshape(E * slots, quarter)
    routed = jnp.zeros((tok_count, quarter), F32)
    for k, pick in enumerate((pick0, pick1)):
        chosen = jnp.where(pick, 1.0, 0.0).astype(BF)
        routed = routed + turned[:, 2 + k : 3 + k] * dot(chosen, outs)

    arrived(sdx.at[: T - 1], s_load.at[0], r_sdx.at[0])
    arrived(hsh.at[: T - 1], s_load.at[0], r_hsh.at[0])
    for q in range(T):
        routed = routed + dot_nt(hsh[q], sdx[q].reshape(K * R, C))
    mixed[...] = routed.astype(BF)

    def gone(ref, sem):
        sent(ref, sem.at[0], sem.at[0])

    gone(tk.at[: T - 1], s_tok)
    gone(hsh.at[: T - 1], s_hsh)
    gone(tok, s_raw)
    gone(meta_send, s_meta)
    gone(gu.at[:G], f_gu)
    gone(gu.at[: E - 1], s_gu)
    gone(dn.at[: K // 2], f_dn)
    gone(ret.at[: G - 1], s_ret)
    gone(port.at[:H], p_in)
    gone(hid.at[:H], s_in)
    gone(sh.at[:G], s_shb)
    gone(sdx.at[: T - 1], s_sdx)
    if H > 1:
        gone(port.at[: H - 1], p_out)
        gone(hid.at[: H - 1], s_out)
    if D > 1:
        gone(disp.at[: D - 1], s_da)

        @pl.when(at_gate)
        def _():
            gone(gw_send, s_gw)

    @pl.when(mine)
    def _():
        gone(dn_send.at[: E - 1], s_dn)

    @pl.when(jnp.logical_not(mine))
    def _():
        gone(dn_send, s_dn)

    def done_groups(d):
        @pl.when((d >= g) & (g > 0))
        def _():
            sent(sh.at[f], s_left.at[d], s_left.at[d])

        @pl.when((d <= g) & (g < G - 1))
        def _():
            sent(sh.at[f], s_right.at[d], s_right.at[d])

    loop(0, G, done_groups)


def hand_on(count, *refs):
    copies = [
        pltpu.make_async_copy(refs[i], refs[count + i], refs[-1].at[i])
        for i in range(count)
    ]
    for copy in copies:
        copy.start()
    for copy in copies:
        copy.wait()


def on_device(
    tokens,
    routes,
    route_weight,
    norm_gain,
    expert_gate,
    expert_up,
    expert_down,
    shared_gate,
    shared_up,
    shared_down,
):
    F = lax.axis_size("fs")
    T = lax.axis_size("tp")
    E, R, C = expert_gate.shape
    tok_count, quarter = tokens.shape
    pick_count = routes.shape[1]
    capacity = 2 * ((3 * tok_count * pick_count + 4 * E - 1) // (4 * E))
    slots = (capacity + 15) // 16 * 16
    G, K = F // 2, F // T
    vmem = pl.BlockSpec(memory_space=pltpu.VMEM)
    hbm = pl.BlockSpec(memory_space=pltpu.HBM)
    dma = pltpu.SemaphoreType.DMA
    shapes = [
        (tok_count, quarter),
        (C // 2, F * R),
        (C // 2, F * R),
        (K * R, T * C // 2),
        (F * R, C),
        (F * R, C),
        (C, F * R),
    ]
    H, D, N = T // 2, G // 2, max(R // 64, 1)
    scratch = [
        (T, tok_count, quarter),
        (T, tok_count, quarter),
        (E, R, 2 * C),
        (F, R, 2 * C),
        (E, R, C),
        (K, T, R, C),
        (F, 3, R, C),
        (D, slots, quarter),
        (T, G, slots, quarter),
        (T, G, slots, C),
        (G, slots, quarter),
        (G, slots, quarter),
        (T, tok_count, C),
        (T, K, R, C),
        (D, tok_count, quarter),
        (D, max(D - 1, 1), slots, quarter),
    ]
    wide = [(8, tok_count), (D, 8, tok_count)]
    one = (1,)
    sems = [
        one, (T,), one, (G, N), one, one, one, (K // 2, T), one, one,
        (G,), (G,), one, (G, 3), (G, 2), one, one, one, (H, G), one,
        one, (D,), one, (D,), one, one, one, (H, G), one, one, one, one, one, one,
    ]
    args = (
        tokens,
        routes.T,
        route_weight.T,
        norm_gain[None, :],
        expert_gate,
        expert_up,
        expert_down,
        shared_gate,
        shared_up,
        shared_down,
    )
    results = pl.pallas_call(
        functools.partial(kernel, F, T, slots),
        out_shape=[jax.ShapeDtypeStruct(s, BF) for s in shapes],
        in_specs=[hbm] * 10,
        out_specs=[vmem] * 7,
        scratch_shapes=[pltpu.VMEM(a.shape, a.dtype) for a in args]
        + [dma((len(args),))]
        + [pltpu.VMEM(s, BF) for s in scratch]
        + [pltpu.VMEM(s, F32) for s in wide]
        + [dma(s) for s in sems],
        compiler_params=pltpu.CompilerParams(
            has_side_effects=True, collective_id=0, vmem_limit_bytes=48 * 1024 * 1024
        ),
    )(*[pltpu.with_memory_space_constraint(a, pltpu.HBM) for a in args])
    mixed, gate, up, down, sg, su, sd = pl.pallas_call(
        functools.partial(hand_on, 7),
        out_shape=[jax.ShapeDtypeStruct(s, BF) for s in shapes],
        in_specs=[vmem] * 7,
        out_specs=[hbm] * 7,
        scratch_shapes=[dma((7,))],
        compiler_params=pltpu.CompilerParams(vmem_limit_bytes=8 * 1024 * 1024),
    )(*results)
    return (mixed, gate.T[None], up.T[None], down[None], sg, su, sd)


def solution(mesh):
    in_specs = (
        P("fs", "tp"),
        P("fs", None),
        P("fs", None),
        P("fs"),
        P(None, "fs", "tp"),
        P(None, "fs", "tp"),
        P(None, "fs", "tp"),
        P("fs", "tp"),
        P("fs", "tp"),
        P("tp", "fs"),
    )
    out_specs = (
        P("fs", "tp"),
        P("fs", None, "tp"),
        P("fs", None, "tp"),
        P("fs", "tp", None),
        P(None, "tp"),
        P(None, "tp"),
        P("tp", None),
    )
    return jax.shard_map(
        on_device, mesh=mesh, in_specs=in_specs, out_specs=out_specs, check_vma=False
    )
```

time: 66.2 us -> 57.8 us (0.87)
  Pallas kernels: 65.4 us -> 57 us
    pallas_call x1, Pallas kernels: 63.9 us -> 55.5 us  [on_device(): pl.pallas_call(functools.partial(kernel, F, T, slots), out_shape=[jax.Sha...]
where the time goes in v3:
time: 57.8 us; the launch traced here: 57.6 us
  Pallas kernels  57 us (99%)
  between operations  0.64 us (1%)
    pallas_call x1, Pallas kernels, on_device(): pl.pallas_call(functools.partial(kernel, F, T, slots), out_shape=[jax.Sha...  55.5 us
    pallas_call x1, Pallas kernels, on_device(): pl.pallas_call(functools.partial(hand_on, 7), out_shape=[jax.ShapeDtypeSt...  1.5 us

profile of v3, /device:TPU:0, one launch (start us, length us, event | category | flops | bytes accessed | tf_op | source)
XLA Modules:
  0.0 57.6 jit_solution(8306326261087202947)
XLA Ops:
  0.6 55.5 %shard_map.153 = (bf16[128,512]{1,0:T(8,128)(2,1)S(1)}, bf16[64,2048]{1,0:T(8,128)(2,1)S(1)}, bf16[64,2048]{1,0:T(8,128)(2,1)S(1)}, bf16[512,256]{1,0:T(8,128)(2...) custom-call(bf16[128,512]{1,0:T(8,128)(2,1)} %tok_in.1, ...), custom_call_target="tpu_custom_call" | custom-call | tf_op jit(solution)/shard_map/pallas_call | solution.py:821
  56.1 1.5 %shard_map.154 = (bf16[128,512]{1,0:T(8,128)(2,1)}, bf16[64,2048]{1,0:T(8,128)(2,1)}, bf16[64,2048]{1,0:T(8,128)(2,1)}, bf16[512,256]{1,0:T(8,128)(2,1)}, bf16[2...) custom-call(bf16[128,512]{1,0:T(8,128)(2,1)S(1)} %get-tuple-element.21.refs_0_, ...), custom_call_target="tpu_custom_call" | custom-call | tf_op jit(solution)/shard_map/pallas_call | solution.py:835

commit v4 on v3

--- a/solution.py
+++ b/solution.py
@@ -311,7 +311,7 @@
                 block // K,
             ).start()
 
-    def relay_right(k):
+    def relay_right(k, low, high, across):
         @pl.when(g - k >= 0)
         def _():
             block = f - 2 * k
@@ -319,12 +319,14 @@
             def piece(i):
                 arrived(sh.at[block, i], s_load.at[0], r_sh.at[block // 2, i])
                 share_right(block, i)
-                share_pair(block, i)
-
-            loop(0, 3, piece)
-            spread(block)
-
-    def relay_left(k):
+                if across:
+                    share_pair(block, i)
+
+            loop(low, high, piece)
+            if low == 0:
+                spread(block)
+
+    def relay_left(k, low, high, across):
         @pl.when(g + k < G)
         def _():
             block = f + 2 * k
@@ -332,28 +334,58 @@
             def piece(i):
                 arrived(sh.at[block, i], s_load.at[0], r_sh.at[block // 2, i])
                 share_left(block, i)
-                share_pair(block, i)
-
-            loop(0, 3, piece)
-            spread(block)
-
-    def relay_in(k):
-        @pl.when(2 * g < G)
-        def _():
-            relay_right(k)
-
-        @pl.when(2 * g >= G)
-        def _():
-            relay_left(k)
-
-    def relay_out(k):
-        @pl.when(2 * g < G)
-        def _():
-            relay_left(k)
-
-        @pl.when(2 * g >= G)
-        def _():
-            relay_right(k)
+                if across:
+                    share_pair(block, i)
+
+            loop(low, high, piece)
+            if low == 0:
+                spread(block)
+
+    def over_right(k):
+        @pl.when(g - k >= 0)
+        def _():
+            loop(0, 3, lambda i: share_pair(f - 2 * k, i))
+
+    def over_left(k):
+        @pl.when(g + k < G)
+        def _():
+            loop(0, 3, lambda i: share_pair(f + 2 * k, i))
+
+    def relay_in(k, low=0, high=3, across=False):
+        @pl.when(left)
+        def _():
+            relay_right(k, low, high, across)
+
+        @pl.when(jnp.logical_not(left))
+        def _():
+            relay_left(k, low, high, across)
+
+    def relay_out(k, low=0, high=3, across=False):
+        @pl.when(left)
+        def _():
+            relay_left(k, low, high, across)
+
+        @pl.when(jnp.logical_not(left))
+        def _():
+            relay_right(k, low, high, across)
+
+    def over_in(k):
+        @pl.when(left)
+        def _():
+            over_right(k)
+
+        @pl.when(jnp.logical_not(left))
+        def _():
+            over_left(k)
+
+    def over_out(k):
+        @pl.when(left)
+        def _():
+            over_left(k)
+
+        @pl.when(jnp.logical_not(left))
+        def _():
+            over_right(k)
 
     for load in loads[2:6]:
         load.wait()
@@ -381,8 +413,23 @@
 
             loop(0, pieces, piece)
 
-    loop(0, E, send_gu)
+    loop(0, D, send_gu)
     gu[f] = gu_send[g]
+
+    for load in loads[6:]:
+        load.wait()
+    sh[f, 0] = sd[...].T.astype(BF)
+    sh[f, 1] = (sg[...] * gains).astype(BF)
+    sh[f, 2] = (su[...] * gains).astype(BF)
+    spread(f)
+    at_end = (g == 0) | (g == G - 1)
+
+    @pl.when(at_end)
+    def _():
+        loop(0, 3, lambda i: share_left(f, i))
+        loop(0, 3, lambda i: share_right(f, i))
+
+    loop(D, E, send_gu)
 
     def cross(src, n):
         remote(
@@ -396,12 +443,6 @@
 
     loop(0, pieces, lambda n: cross(f, n))
 
-    for load in loads[6:]:
-        load.wait()
-    sh[f, 0] = sd[...].T.astype(BF)
-    sh[f, 1] = (sg[...] * gains).astype(BF)
-    sh[f, 2] = (su[...] * gains).astype(BF)
-    spread(f)
     loop(0, 3, lambda i: share_pair(f, i))
 
     def take_block(group):
@@ -493,18 +534,6 @@
         ).start()
 
 
-    def hand_across(i):
-        k = 2 * i + p
-
-        def chunk(q):
-            @pl.when(jnp.logical_not((t * K + k == f) & (q == t)))
-            def _():
-                arrived(dn.at[k, q], s_load.at[0], r_dn.at[i, q])
-
-            remote(dn.at[k, q], dn.at[k, q], f_dn.at[0], x_dn.at[0], pair, t).start()
-
-        loop(0, T, chunk)
-
     def pass_hidden(i):
         group = near_first(i)
         for o in range(1, H):
@@ -520,6 +549,11 @@
             ).start()
 
 
+    def send_ret(group):
+        remote(
+            ret_send.at[group], ret.at[g], s_ret.at[0], r_ret.at[0], 2 * group + p, t
+        ).start()
+
     def expert_out(i):
         group = near_first(i)
         arrived(hid.at[:H, group], s_load.at[0], r_hid.at[0, group])
@@ -528,11 +562,9 @@
             total = total + dot_nt(hid[q, group], dn[:, q].reshape(K * R, C))
         ret_send[group] = total.astype(BF)
 
-        @pl.when(group != g)
-        def _():
-            remote(
-                ret_send.at[group], ret.at[g], s_ret.at[0], r_ret.at[0], 2 * group + p, t
-            ).start()
+        @pl.when((group != g) & (i < G - 1))
+        def _():
+            send_ret(group)
 
 
     at_gate = depth == D - 1
@@ -559,20 +591,43 @@
     def _():
         dn[f % K, t] = dn_send[g]
 
-    loop(0, 3, lambda i: share_left(f, i))
-    loop(0, 3, lambda i: share_right(f, i))
-
+    @pl.when(jnp.logical_not(at_end))
+    def _():
+        loop(0, 3, lambda i: share_left(f, i))
+        loop(0, 3, lambda i: share_right(f, i))
+
+
+    def hand_across(i):
+        k = 2 * i + p
+
+        def chunk(q):
+            @pl.when(jnp.logical_not((t * K + k == f) & (q == t)))
+            def _():
+                arrived(dn.at[k, q], s_load.at[0], r_dn.at[i, q])
+
+            remote(dn.at[k, q], dn.at[k, q], f_dn.at[0], x_dn.at[0], pair, t).start()
+
+        loop(0, T, chunk)
 
     loop(0, G // 2, take_near)
+    loop(1, G // 2, relay_in)
+    loop(1, G // 2, over_in)
+    loop(0, pieces // 2, take_far)
 
     @pl.when(jnp.logical_not(at_gate))
     def _():
         loop(0, D, lambda i: take_other(D - 1 - i))
 
-    loop(0, pieces, take_far)
+    loop(pieces // 2, pieces, take_far)
+    @pl.when(at_end)
+    def _():
+        loop(0, K // 2, hand_across)
+
     loop(0, G, inner_block)
-    loop(0, K // 2, hand_across)
-    loop(1, G // 2, relay_in)
+    @pl.when(jnp.logical_not(at_end))
+    def _():
+        loop(0, K // 2, hand_across)
+
 
     for o in range(1, H):
         src = (t + 2 * o) % T
@@ -591,24 +646,30 @@
     arrived(port.at[:H], s_load.at[0], x_port.at[0])
     arrived(gu.at[:G], s_load.at[0], x_gu.at[0])
     loop(0, G, expert_hidden)
-    loop(1, min(2, G), relay_out)
+    loop(1, min(2, G), lambda k: relay_out(k, across=True))
     loop(0, G, pass_hidden)
-    at_end = (g == 0) | (g == G - 1)
-
     @pl.when(jnp.logical_not(at_end))
     def _():
         loop(2, G // 2 + 1, relay_out)
+        loop(2, G // 2 + 1, over_out)
+
+    @pl.when(at_end)
+    def _():
+        loop(2, G // 2 + 1, lambda k: relay_out(k, across=True))
 
     arrived(dn.at[: K // 2], s_load.at[0], x_dn.at[0])
     loop(0, G, expert_out)
     ret[g] = ret_send[g]
 
-    @pl.when(at_end)
-    def _():
-        loop(2, G // 2 + 1, relay_out)
-
-    loop(G // 2 + 1, G, relay_out)
-    loop(G // 2, G, relay_in)
+
+    def late_out(k):
+        relay_out(k, across=True)
+
+    def late_in(k):
+        relay_in(k, across=True)
+
+    loop(G // 2 + 1, G, late_out)
+    loop(G // 2, G, late_in)
 
     def place_down(k):
         for q in range(0, T, 2):
@@ -626,6 +687,7 @@
         spread(block)
         arrived(sh.at[block, 1:3], s_load.at[0], r_shp.at[block // 2, 1])
 
+    send_ret(near_first(G - 1))
     loop(0, G, wait_down)
 
     gate_sh = sh[:, 1].reshape(F * R, C)

time: 57.8 us -> 55.1 us (0.953)
  Pallas kernels: 57 us -> 54.3 us
    pallas_call x1, Pallas kernels: 55.5 us -> 52.8 us  [on_device(): pl.pallas_call(functools.partial(kernel, F, T, slots), out_shape=[jax.Sha...]
where the time goes in v4:
time: 55.1 us; the launch traced here: 55 us
  Pallas kernels  54.3 us (99%)
  between operations  0.64 us (1%)
    pallas_call x1, Pallas kernels, on_device(): pl.pallas_call(functools.partial(kernel, F, T, slots), out_shape=[jax.Sha...  52.8 us
    pallas_call x1, Pallas kernels, on_device(): pl.pallas_call(functools.partial(hand_on, 7), out_shape=[jax.ShapeDtypeSt...  1.5 us

profile of v4, /device:TPU:0, one launch (start us, length us, event | category | flops | bytes accessed | tf_op | source)
XLA Modules:
  0.0 55.0 jit_solution(18102972576831383181)
XLA Ops:
  0.6 52.8 %shard_map.153 = (bf16[128,512]{1,0:T(8,128)(2,1)S(1)}, bf16[64,2048]{1,0:T(8,128)(2,1)S(1)}, bf16[64,2048]{1,0:T(8,128)(2,1)S(1)}, bf16[512,256]{1,0:T(8,128)(2...) custom-call(bf16[128,512]{1,0:T(8,128)(2,1)} %tok_in.1, ...), custom_call_target="tpu_custom_call" | custom-call | tf_op jit(solution)/shard_map/pallas_call | solution.py:883
  53.5 1.5 %shard_map.154 = (bf16[128,512]{1,0:T(8,128)(2,1)}, bf16[64,2048]{1,0:T(8,128)(2,1)}, bf16[64,2048]{1,0:T(8,128)(2,1)}, bf16[512,256]{1,0:T(8,128)(2,1)}, bf16[2...) custom-call(bf16[128,512]{1,0:T(8,128)(2,1)S(1)} %get-tuple-element.21.refs_0_, ...), custom_call_target="tpu_custom_call" | custom-call | tf_op jit(solution)/shard_map/pallas_call | solution.py:897

commit v5 on v4

--- a/solution.py
+++ b/solution.py
@@ -842,7 +842,7 @@
         (F * R, C),
         (C, F * R),
     ]
-    H, D, N = T // 2, G // 2, max(R // 64, 1)
+    H, D, N = T // 2, G // 2, max(R // 128, 1)
     scratch = [
         (T, tok_count, quarter),
         (T, tok_count, quarter),

time: 55.1 us -> 55 us (level)
  no operation moved by 1% of the time
where the time goes in v5:
time: 55 us; the launch traced here: 54.9 us
  Pallas kernels  54.2 us (99%)
  between operations  0.64 us (1%)
    pallas_call x1, Pallas kernels, on_device(): pl.pallas_call(functools.partial(kernel, F, T, slots), out_shape=[jax.Sha...  52.7 us
    pallas_call x1, Pallas kernels, on_device(): pl.pallas_call(functools.partial(hand_on, 7), out_shape=[jax.ShapeDtypeSt...  1.5 us

profile of v5, /device:TPU:0, one launch (start us, length us, event | category | flops | bytes accessed | tf_op | source)
XLA Modules:
  0.0 54.9 jit_solution(13402552730891257157)
XLA Ops:
  0.6 52.7 %shard_map.153 = (bf16[128,512]{1,0:T(8,128)(2,1)S(1)}, bf16[64,2048]{1,0:T(8,128)(2,1)S(1)}, bf16[64,2048]{1,0:T(8,128)(2,1)S(1)}, bf16[512,256]{1,0:T(8,128)(2...) custom-call(bf16[128,512]{1,0:T(8,128)(2,1)} %tok_in.1, ...), custom_call_target="tpu_custom_call" | custom-call | tf_op jit(solution)/shard_map/pallas_call | solution.py:883
  53.4 1.5 %shard_map.154 = (bf16[128,512]{1,0:T(8,128)(2,1)}, bf16[64,2048]{1,0:T(8,128)(2,1)}, bf16[64,2048]{1,0:T(8,128)(2,1)}, bf16[512,256]{1,0:T(8,128)(2,1)}, bf16[2...) custom-call(bf16[128,512]{1,0:T(8,128)(2,1)S(1)} %get-tuple-element.21.refs_0_, ...), custom_call_target="tpu_custom_call" | custom-call | tf_op jit(solution)/shard_map/pallas_call | solution.py:897
